TPU v7x, 32 devices: a whole 2x2x4 slice. The times are simulated.
32 devices in a mesh: sp: 8 (over z, x), tp: 4 (over y, core).
Axes of the slice: x: 2, y: 2, z: 4, core: 2. Of those that a mesh axis runs over, the one named last changes fastest.
Arguments:
- residual_in: bfloat16 [1024, 2048], P('sp', 'tp'), may hold values from -8 to 8
- query_alpha: bfloat16 [1024, 2048], P('sp', 'tp'), may hold values from -8 to 8
- pairs_alpha: bfloat16 [1024, 16, 128], P('sp', 'tp'), may hold values from -8 to 8
- offset_alpha: float32 [1024, 32], P('sp', 'tp'), may hold values from -18 to -1
- gain_alpha: float32 [2048], P('tp'), may hold values from 0.1 to 1.9
- query_beta: bfloat16 [1024, 2048], P('sp', 'tp'), may hold values from -8 to 8
- pairs_beta: bfloat16 [1024, 16, 256], P('sp', 'tp'), may hold values from -8 to 8
- offset_beta: float32 [1024, 16], P('sp', 'tp'), may hold values from -18 to -1
- gain_beta: float32 [2048], P('tp'), may hold values from 0.1 to 1.9
- project_alpha: bfloat16 [2048, 2048], P('tp'), may hold values from -0.09375 to 0.09375
- project_beta: bfloat16 [2048, 2048], P('tp'), may hold values from -0.09375 to 0.09375
- gain_settle: float32 [2048], P('tp'), may hold values from 0 to 4
- bias_settle: float32 [2048], P('tp'), may hold values from -2.5 to 2.5
- expert_ids: int32 [1024, 2], P('sp'), may hold values from 0 to 7, as said below
- route_weight: float32 [1024, 2], P('sp'), may hold values from 0.1 to 0.9
- expert_gate: bfloat16 [8, 2048, 4096], P('sp', None, 'tp'), may hold values from -0.125 to 0.125
- expert_up: bfloat16 [8, 2048, 4096], P('sp', None, 'tp'), may hold values from -0.125 to 0.125
- expert_down: bfloat16 [8, 4096, 2048], P('sp', 'tp'), may hold values from -0.1875 to 0.1875
- gain_final: float32 [2048], P('tp'), may hold values from 0.1 to 1.9
- bias_final: float32 [2048], P('tp'), may hold values from -2.5 to 2.5
Outputs:
- layer_out: bfloat16 [1024, 2048], P('sp', 'tp')
Inputs may be any that keep to these rules, and one draw needn't show every extreme that they name: `expert_ids`: the two numbers of a row differ and lie in one group of 2 consecutive experts. Among the rows of one device, no expert is named more than 48 times, and every expert of one group, the same group for all devices, is named exactly 48 times.
All inputs are finite; a program needn't handle non-finite values.
Results may differ from a plain program's by a relative error of at most 0.018.
Values may be sent and summed in bfloat16 or wider, within the bound.
A program may use at most 64 MiB of HBM per device.

v0:
```python
import functools
import jax
import jax.numpy as jnp
from jax import lax
from jax.experimental import pallas as pl
from jax.experimental.pallas import tpu as pltpu
from jax.sharding import PartitionSpec as P

depth_scale = 2.0**0.5
norm_eps = 1e-05
F32 = jnp.float32
BF16 = jnp.bfloat16
VMEM = pltpu.VMEM
DMA = pltpu.SemaphoreType.DMA


def remote(src, dst, send, recv, where):
    return pltpu.make_async_remote_copy(
        src_ref=src,
        dst_ref=dst,
        send_sem=send,
        recv_sem=recv,
        device_id=where,
        device_id_type=pl.DeviceIdType.MESH,
    )


def greet(n_sp, n_tp, sp, tp):
    barrier = pltpu.get_barrier_semaphore()
    for o in range(1, n_sp):
        pl.semaphore_signal(
            barrier,
            inc=1,
            device_id={"sp": lax.rem(sp + o, n_sp), "tp": tp},
            device_id_type=pl.DeviceIdType.MESH,
        )
    for o in range(1, n_tp):
        pl.semaphore_signal(
            barrier,
            inc=1,
            device_id={"sp": sp, "tp": lax.rem(tp + o, n_tp)},
            device_id_type=pl.DeviceIdType.MESH,
        )
    pl.semaphore_wait(barrier, n_sp + n_tp - 2)


def split(x):
    high = x.astype(BF16)
    return high, (x - high.astype(F32)).astype(BF16)


def lane_sums(x):
    ones = jnp.ones((8, x.shape[1]), BF16)
    dims = (((1,), (1,)), ((), ()))
    high, low = split(x)
    return lax.dot_general(ones, high, dims, preferred_element_type=F32) + lax.dot_general(
        ones, low, dims, preferred_element_type=F32
    )


def column(row, rows):
    return jnp.transpose(jnp.broadcast_to(row[0:1, :], (rows, rows)))[:, 0:1]


def stats_start(n_tp, sp, tp, one, two, stat, send, recv):
    stat[tp, 0] = one
    stat[tp, 1] = two
    for o in range(1, n_tp):
        remote(
            stat.at[tp], stat.at[tp], send.at[o], recv.at[tp], {"sp": sp, "tp": lax.rem(tp + o, n_tp)}
        ).start()


def stats_finish(n_tp, sp, tp, stat, send, recv, rows):
    for o in range(1, n_tp):
        peer = lax.rem(tp + o, n_tp)
        remote(stat.at[peer], stat.at[peer], send.at[o], recv.at[peer], {"sp": sp, "tp": peer}).wait_recv()
    for o in range(1, n_tp):
        peer = lax.rem(tp + o, n_tp)
        remote(stat.at[tp], stat.at[tp], send.at[o], recv.at[tp], {"sp": sp, "tp": peer}).wait_send()
    total = stat[0]
    for t in range(1, n_tp):
        total = total + stat[t]
    return column(total[0], rows), column(total[1], rows)


def norm(total, one, two, gain, bias, columns):
    mean = one / columns
    var = two / columns - mean * mean
    return ((total - mean) * lax.rsqrt(var + norm_eps) * gain + bias).astype(BF16)


def attend_kernel(
    early,
    n_sp,
    n_tp,
    nx,
    kva,
    kvb,
    qa_ref,
    qb_ref,
    kva_hbm,
    kvb_hbm,
    off_hbm,
    res_ref,
    ga_ref,
    gb_ref,
    pa_hbm,
    pb_hbm,
    gs_ref,
    bs_ref,
    out_ref,
    kvbuf,
    offbuf,
    qs,
    acc,
    rem,
    pa,
    pb,
    ya,
    yb,
    part,
    got,
    stat1,
    stat2,
    load_sem,
    kv_send,
    kv_recv,
    off_send,
    off_recv,
    part_send,
    part_recv,
    s1_send,
    s1_recv,
    s2_send,
    s2_recv,
):
    sp = lax.axis_index("sp")
    tp = lax.axis_index("tp")
    nz = n_sp // nx
    z = sp // nx
    x = lax.rem(sp, nx)
    rows = qa_ref.shape[0]
    cols = out_ref.shape[1]
    loads = (
        pltpu.make_async_copy(kva_hbm, kvbuf.at[sp, :, 0 : kva * 128], load_sem.at[0]),
        pltpu.make_async_copy(off_hbm, offbuf.at[sp], load_sem.at[1]),
        pltpu.make_async_copy(pa_hbm, pa, load_sem.at[2]),
        pltpu.make_async_copy(pb_hbm, pb, load_sem.at[3]),
        pltpu.make_async_copy(kvb_hbm, kvbuf.at[sp, :, kva * 128 :], load_sem.at[4]),
    )
    for load in loads:
        load.start()
    greet(n_sp, n_tp, sp, tp)
    lane = lax.broadcasted_iota(jnp.int32, (rows, 128), 1)
    row_i = lax.broadcasted_iota(jnp.int32, (rows, 128), 0)
    first_half = lane < 64
    for u in range(kva):
        q32 = qa_ref[:, u * 128 : (u + 1) * 128].astype(F32) * (64**-0.5)
        qs[u, 0:rows] = jnp.where(first_half, q32, 0.0).astype(BF16)
        qs[u, rows : 2 * rows] = jnp.where(first_half, pltpu.roll(q32, 64, 1), 0.0).astype(BF16)
    acc[...] = jnp.zeros_like(acc)
    rem[...] = jnp.zeros_like(rem)
    tri_r = lax.broadcasted_iota(jnp.int32, (256, 256), 0) % 128
    tri_c = lax.broadcasted_iota(jnp.int32, (256, 256), 1)
    tri = jnp.where((tri_r > tri_c) | (tri_c >= 128), 1.0, 0.0).astype(BF16)

    def block(j):
        gap = (sp - j) * rows
        valid1 = lane < row_i + gap
        valid2 = jnp.concatenate([valid1.astype(F32)] * 2, axis=0) > 0.5

        def unit(query, key, value, offset, scale, valid, left):
            s = lax.dot_general(query, key, (((1,), (1,)), ((), ())), preferred_element_type=F32)
            s = (s if scale is None else s * scale) + offset
            soft = jnp.maximum(s, 0.0) + jnp.log(1.0 + jnp.exp(-jnp.abs(s)))
            used = jnp.where(valid, soft, 0.0)
            high, low = split(used)
            sums = jnp.dot(jnp.concatenate([high, low], axis=1), tri, preferred_element_type=F32)
            w = jnp.where(valid, jnp.exp(s - soft - sums[:, :128] + left), 0.0).astype(BF16)
            return jnp.dot(w, value, preferred_element_type=F32), sums[:, 128:]

        for u in range(kva):
            pair = kvbuf[j, :, u * 128 : (u + 1) * 128]
            offset = jnp.concatenate(
                [
                    jnp.broadcast_to(offbuf[j, 2 * u : 2 * u + 1, :], (rows, 128)),
                    jnp.broadcast_to(offbuf[j, 2 * u + 1 : 2 * u + 2, :], (rows, 128)),
                ],
                axis=0,
            )
            left = rem[2 * u * rows : (2 * u + 2) * rows]
            o, total = unit(qs[u], pair, pair, offset, None, valid2, left)
            rem[2 * u * rows : (2 * u + 2) * rows] = left - total
            acc[:, u * 128 : (u + 1) * 128] += jnp.where(
                first_half, pltpu.roll(o[:rows], 64, 1), o[rows:]
            )
        for u in range(kvb):
            base = kva * 128 + u * 256
            head = 2 * kva + u
            key = kvbuf[j, :, base : base + 128]
            value = kvbuf[j, :, base + 128 : base + 256]
            offset = offbuf[j, head : head + 1, :]
            left = rem[head * rows : (head + 1) * rows]
            query = qb_ref[:, u * 128 : (u + 1) * 128]
            o, total = unit(query, key, value, offset, 128**-0.5, valid1, left)
            rem[head * rows : (head + 1) * rows] = left - total
            c = (kva + u) * 128
            acc[:, c : c + 128] += o

    def sends(s):
        j0 = (z - s) * nx + x
        plan = [(z + 1 < nz, jnp.minimum(z + 1, nz - 1) * nx + x)]
        for d in range(1, nx):
            xo = lax.rem(x + d, nx)
            plan.append(((s > 0) | (x < xo), z * nx + xo))
        made = []
        for k, (cond, dest) in enumerate(plan):
            where = {"sp": dest, "tp": tp}
            made.append(
                (
                    cond,
                    remote(kvbuf.at[j0], kvbuf.at[j0], kv_send.at[s, k], kv_recv.at[j0], where),
                    remote(offbuf.at[j0], offbuf.at[j0], off_send.at[s, k], off_recv.at[j0], where),
                )
            )
        return made

    def wait_block(j):
        where = {"sp": sp, "tp": tp}
        remote(kvbuf.at[j], kvbuf.at[j], kv_send.at[0, 0], kv_recv.at[j], where).wait_recv()
        remote(offbuf.at[j], offbuf.at[j], off_send.at[0, 0], off_recv.at[j], where).wait_recv()

    loads[0].wait()
    loads[1].wait()
    loads[4].wait()

    def forward(s):
        @pl.when(s > 0)
        def _():
            wait_block((z - s) * nx + x)

        for cond, kv_copy, off_copy in sends(s):

            @pl.when(cond)
            def _(kv_copy=kv_copy, off_copy=off_copy):
                off_copy.start()
                kv_copy.start()

    forward(0)

    def level(s, carry):
        src = z - s

        @pl.when(s < z)
        def _():
            forward(s + 1)

        def across(i, inner):
            xo = nx - 1 - i

            @pl.when((s > 0) | (xo <= x))
            def _():
                @pl.when(xo != x)
                def _():
                    wait_block(src * nx + xo)

                block(src * nx + xo)

            return inner

        return lax.fori_loop(0, nx, across, carry)

    lax.fori_loop(0, z + 1, level, 0)
    early()

    wide = kva * 128
    aa = acc[:, :wide]
    ab = acc[:, wide:]
    stats_start(n_tp, sp, tp, lane_sums(aa * aa), lane_sums(ab * ab), stat1, s1_send, s1_recv)
    loads[2].wait()
    loads[3].wait()
    na = (aa * ga_ref[...]).astype(BF16)
    nb = (ab * gb_ref[...]).astype(BF16)
    for t in range(n_tp):
        ya[t] = jnp.dot(na, pa[:, t * cols : (t + 1) * cols], preferred_element_type=F32)
        yb[t] = jnp.dot(nb, pb[:, t * cols : (t + 1) * cols], preferred_element_type=F32)
    sq_a, sq_b = stats_finish(n_tp, sp, tp, stat1, s1_send, s1_recv, rows)
    scale_a = lax.rsqrt(sq_a / (wide * n_tp) + norm_eps)
    scale_b = lax.rsqrt(sq_b / (kvb * 128 * n_tp) + norm_eps)

    def part_copy(o):
        peer = lax.rem(tp + o, n_tp)
        return remote(
            part.at[peer], got.at[tp], part_send.at[o], part_recv.at[tp], {"sp": sp, "tp": peer}
        )

    for o in range(1, n_tp):
        peer = lax.rem(tp + o, n_tp)
        part[peer] = (ya[peer] * scale_a + yb[peer] * scale_b).astype(BF16)
        part_copy(o).start()
    total = (ya[tp] * scale_a + yb[tp] * scale_b).astype(BF16).astype(F32)
    for o in range(1, n_tp):
        peer = lax.rem(tp + o, n_tp)
        remote(
            part.at[peer], got.at[peer], part_send.at[o], part_recv.at[peer], {"sp": sp, "tp": peer}
        ).wait_recv()
        total = total + got[peer].astype(F32)
    mixed = total.astype(BF16).astype(F32)
    first = depth_scale * res_ref[...].astype(F32) + mixed
    stats_start(n_tp, sp, tp, lane_sums(first), lane_sums(first * first), stat2, s2_send, s2_recv)
    for o in range(1, n_tp):
        part_copy(o).wait_send()

    def drain(s, carry):
        for cond, kv_copy, off_copy in sends(s):

            @pl.when(cond)
            def _(kv_copy=kv_copy, off_copy=off_copy):
                off_copy.wait_send()
                kv_copy.wait_send()

        return carry

    lax.fori_loop(0, z + 1, drain, 0)
    one, two = stats_finish(n_tp, sp, tp, stat2, s2_send, s2_recv, rows)
    out_ref[...] = norm(first, one, two, gs_ref[...], bs_ref[...], cols * n_tp)


def expert_kernel(
    attention,
    n_sp,
    n_tp,
    nx,
    cap,
    set_ref,
    ids_ref,
    wg_hbm,
    wu_hbm,
    wd_hbm,
    gf_ref,
    bf_ref,
    out_ref,
    wg,
    wu,
    wd,
    sendbuf,
    xbuf,
    gate,
    up,
    hid,
    away,
    arrived,
    home,
    pre,
    peers,
    outb,
    back,
    stat,
    load_sem,
    a_send,
    a_recv,
    x_send,
    x_recv,
    relay_send,
    d_send,
    d_recv,
    y_send,
    y_recv,
    b_send,
    b_recv,
    s_send,
    s_recv,
):
    sp = lax.axis_index("sp")
    tp = lax.axis_index("tp")
    rows, cols = set_ref.shape
    places = n_sp * cap
    ny = n_tp // 2
    y = tp // 2
    core = lax.rem(tp, 2)
    mate = y * 2 + 1 - core
    loads = (
        pltpu.make_async_copy(wg_hbm.at[0], wg, load_sem.at[0]),
        pltpu.make_async_copy(wu_hbm.at[0], wu, load_sem.at[1]),
        pltpu.make_async_copy(wd_hbm.at[0], wd, load_sem.at[2]),
    )

    def loop(low, high, fn):
        def step(i, carry):
            fn(i)
            return carry

        lax.fori_loop(low, high, step, 0)

    def x_copies(j):
        made = []
        for k in range(ny):
            dest = mate if k == 0 else lax.rem(y + k, ny) * 2 + core
            made.append(
                remote(
                    xbuf.at[tp, j], xbuf.at[tp, j], x_send.at[k, j], x_recv.at[tp, j], {"sp": sp, "tp": dest}
                )
            )
        return made

    def spread_out(j):
        @pl.when(j != sp)
        def _():
            remote(
                sendbuf.at[j], xbuf.at[tp, j], a_send.at[0], a_recv.at[j], {"sp": sp, "tp": tp}
            ).wait_recv()

        for copy in x_copies(j):
            copy.start()

    ahead = jnp.maximum(sp // nx - 1, 0) * nx

    for load in loads:
        load.start()
    attention(lambda: loop(0, ahead, spread_out))
    ids = ids_ref[...][:, 0:2]
    expert = lax.broadcasted_iota(jnp.int32, (rows, 128), 1).astype(F32)
    hot = [jnp.where(ids[:, k : k + 1] == expert, 1.0, 0.0) for k in range(2)]
    r = lax.broadcasted_iota(jnp.int32, (rows, rows), 0)
    c = lax.broadcasted_iota(jnp.int32, (rows, rows), 1)
    lower = jnp.where(c < r, 1.0, 0.0).astype(BF16)
    before = jnp.dot(lower, (hot[0] + hot[1]).astype(BF16), preferred_element_type=F32)
    seat = lax.broadcasted_iota(jnp.int32, (rows, places), 1).astype(F32)
    hits = []
    for k in range(2):
        slot = jnp.sum(before * hot[k], axis=1, keepdims=True)
        place = ids[:, k : k + 1] * cap + slot
        hits.append(jnp.where(place == seat, 1.0, 0.0))
    spread = jnp.transpose(hits[0] + hits[1]).astype(BF16)
    sent = jnp.dot(spread, set_ref[...], preferred_element_type=F32).astype(BF16)
    sendbuf[...] = sent.reshape(n_sp, cap, cols)

    def at_sp(o):
        return lax.rem(sp + o, n_sp)

    def a_copy(o):
        dest = at_sp(o)
        return remote(
            sendbuf.at[dest], xbuf.at[tp, sp], a_send.at[o], a_recv.at[sp], {"sp": dest, "tp": tp}
        )

    loop(1, n_sp, lambda o: a_copy(o).start())
    xbuf[tp, sp] = sendbuf[sp]

    def x_wait(t, j):
        remote(xbuf.at[t, j], xbuf.at[t, j], x_send.at[0, 0], x_recv.at[t, j], {"sp": sp, "tp": t}).wait_recv()

    loop(ahead, n_sp, spread_out)

    def relay_copy(k, o):
        t = lax.rem(y + k, ny) * 2 + core
        j = o
        return remote(
            xbuf.at[t, j], xbuf.at[t, j], relay_send.at[k, o], x_recv.at[t, j], {"sp": sp, "tp": mate}
        )

    def gather_dot(t, fresh):
        xs = xbuf[t].reshape(places, cols)
        at = pl.ds(pl.multiple_of(t * cols, 128), cols)
        g = jnp.dot(xs, wg[at, :], preferred_element_type=F32)
        u = jnp.dot(xs, wu[at, :], preferred_element_type=F32)
        if fresh:
            gate[...] = g
            up[...] = u
        else:
            gate[...] += g
            up[...] += u

    loads[0].wait()
    loads[1].wait()
    gather_dot(tp, True)

    def arrive_mate(o):
        x_wait(mate, o)

    loop(0, n_sp, arrive_mate)
    gather_dot(mate, False)

    def from_y(k):
        t = lax.rem(y + k, ny) * 2 + core
        other = lax.rem(y + k, ny) * 2 + 1 - core

        def pass_on(o):
            x_wait(t, o)
            relay_copy(k, o).start()

        loop(0, n_sp, pass_on)
        gather_dot(t, False)

        def arrive(o):
            x_wait(other, o)

        loop(0, n_sp, arrive)
        gather_dot(other, False)

    loop(1, ny, from_y)
    value = gate[...]
    hid[...] = (value / (1.0 + jnp.exp(-value)) * up[...]).astype(BF16)
    loads[2].wait()

    def down(t):
        at = pl.ds(pl.multiple_of(t * cols, 128), cols)
        result = jnp.dot(hid[...], wd[:, at], preferred_element_type=F32)
        return result.astype(BF16).reshape(n_sp, cap, cols)

    def d_copy(k):
        return remote(away.at[k], arrived.at[k], d_send.at[k], d_recv.at[k], {"sp": sp, "tp": mate})

    def down_away(i):
        k = lax.rem(i + 1, ny)
        away[k] = down(lax.rem(y + k, ny) * 2 + 1 - core)
        d_copy(k).start()

    loop(0, ny, down_away)

    def down_home(i):
        k = lax.rem(i + 1, ny)
        home[k] = down(lax.rem(y + k, ny) * 2 + core)

    loop(0, ny, down_home)

    def y_copy(k, o):
        j = at_sp(o)
        return remote(
            pre.at[k, j],
            peers.at[k, j],
            y_send.at[k, o],
            y_recv.at[k, j],
            {"sp": sp, "tp": lax.rem(y + k, ny) * 2 + core},
        )

    for i in range(ny):
        k = (i + 1) % ny
        d_copy(k).wait_recv()
        if k:

            def to_y(o, k=k):
                j = at_sp(o)
                pre[k, j] = (home[k, j].astype(F32) + arrived[k, j].astype(F32)).astype(BF16)
                y_copy(k, o).start()

            loop(1, n_sp, to_y)
            to_y(0)

    def b_copy(o):
        dest = at_sp(o)
        return remote(outb.at[dest], back.at[sp], b_send.at[o], b_recv.at[sp], {"sp": dest, "tp": tp})

    def settle(o):
        j = at_sp(o)
        total = home[0, j].astype(F32) + arrived[0, j].astype(F32)
        for k in range(1, ny):
            remote(
                pre.at[k, j], peers.at[k, j], y_send.at[k, 0], y_recv.at[k, j], {"sp": sp, "tp": mate}
            ).wait_recv()
            total = total + peers[k, j].astype(F32)
        return total.astype(BF16)

    def give_back(o):
        outb[at_sp(o)] = settle(o)
        b_copy(o).start()

    loop(1, n_sp, give_back)
    back[sp] = settle(0)

    def wait_back(o):
        j = lax.rem(sp - o + n_sp, n_sp)
        remote(outb.at[j], back.at[j], b_send.at[0], b_recv.at[j], {"sp": j, "tp": tp}).wait_recv()

    loop(1, n_sp, wait_back)
    flat = back[...].reshape(places, cols)
    weight = ids_ref[...][:, 2:4]
    routed = weight[:, 0:1] * jnp.dot(hits[0].astype(BF16), flat, preferred_element_type=F32)
    routed = routed + weight[:, 1:2] * jnp.dot(hits[1].astype(BF16), flat, preferred_element_type=F32)
    second = depth_scale * set_ref[...].astype(F32) + routed
    stats_start(n_tp, sp, tp, lane_sums(second), lane_sums(second * second), stat, s_send, s_recv)

    def drain(o):
        for copy in x_copies(o):
            copy.wait_send()
        for k in range(1, ny):
            relay_copy(k, o).wait_send()
            y_copy(k, o).wait_send()

    loop(0, n_sp, drain)

    def drain_sp(o):
        a_copy(o).wait_send()
        b_copy(o).wait_send()

    loop(1, n_sp, drain_sp)
    for k in range(ny):
        d_copy(k).wait_send()
    one, two = stats_finish(n_tp, sp, tp, stat, s_send, s_recv, rows)
    out_ref[...] = norm(second, one, two, gf_ref[...], bf_ref[...], cols * n_tp)


def body(
    residual_in,
    query_alpha,
    pairs_alpha,
    offset_alpha,
    gain_alpha,
    query_beta,
    pairs_beta,
    offset_beta,
    gain_beta,
    project_alpha,
    project_beta,
    gain_settle,
    bias_settle,
    expert_ids,
    route_weight,
    expert_gate,
    expert_up,
    expert_down,
    gain_final,
    bias_final,
):
    n_sp = lax.axis_size("sp")
    n_tp = lax.axis_size("tp")
    nx = 2 ** ((n_sp.bit_length() - 1) // 2)
    nz = n_sp // nx
    rows, cols = residual_in.shape
    kva = pairs_alpha.shape[1]
    kvb = pairs_beta.shape[1]
    heads = 2 * kva + kvb
    heads_pad = -(-heads // 8) * 8
    off = jnp.transpose(jnp.concatenate([offset_alpha, offset_beta], axis=1))
    off = jnp.pad(off, ((0, heads_pad - heads), (0, 0)))
    kv_cols = kva * 128 + kvb * 256
    inner = kva * 128
    inner_b = kvb * 128
    vm = pl.BlockSpec(memory_space=VMEM)
    hbm = pl.BlockSpec(memory_space=pl.ANY)
    row = lambda v: v.reshape(1, -1)
    cap = -(-(3 * rows // n_sp) // 16) * 16
    places = n_sp * cap
    ny = n_tp // 2
    width, units = expert_gate.shape[1:]
    attend_scratch = [
        VMEM((n_sp, rows, kv_cols), BF16),
        VMEM((n_sp, heads_pad, rows), F32),
        VMEM((kva, 2 * rows, 128), BF16),
        VMEM((rows, inner + inner_b), F32),
        VMEM((heads * rows, 128), F32),
        VMEM(project_alpha.shape, BF16),
        VMEM(project_beta.shape, BF16),
        VMEM((n_tp, rows, cols), F32),
        VMEM((n_tp, rows, cols), F32),
        VMEM((n_tp, rows, cols), BF16),
        VMEM((n_tp, rows, cols), BF16),
        VMEM((n_tp, 2, 8, rows), F32),
        VMEM((n_tp, 2, 8, rows), F32),
        DMA((5,)),
        DMA((nz, nx)),
        DMA((n_sp,)),
        DMA((nz, nx)),
        DMA((n_sp,)),
        DMA((n_tp,)),
        DMA((n_tp,)),
        DMA((n_tp,)),
        DMA((n_tp,)),
        DMA((n_tp,)),
        DMA((n_tp,)),
    ]
    expert_scratch = [
        VMEM((width, units), BF16),
        VMEM((width, units), BF16),
        VMEM((units, width), BF16),
        VMEM((n_sp, cap, cols), BF16),
        VMEM((n_tp, n_sp, cap, cols), BF16),
        VMEM((places, units), F32),
        VMEM((places, units), F32),
        VMEM((places, units), BF16),
        VMEM((ny, n_sp, cap, cols), BF16),
        VMEM((ny, n_sp, cap, cols), BF16),
        VMEM((ny, n_sp, cap, cols), BF16),
        VMEM((ny, n_sp, cap, cols), BF16),
        VMEM((ny, n_sp, cap, cols), BF16),
        VMEM((n_sp, cap, cols), BF16),
        VMEM((n_sp, cap, cols), BF16),
        VMEM((n_tp, 2, 8, rows), F32),
        DMA((3,)),
        DMA((n_sp,)),
        DMA((n_sp,)),
        DMA((ny, n_sp)),
        DMA((n_tp, n_sp)),
        DMA((ny, n_sp)),
        DMA((ny,)),
        DMA((ny,)),
        DMA((ny, n_sp)),
        DMA((ny, n_sp)),
        DMA((n_sp,)),
        DMA((n_sp,)),
        DMA((n_tp,)),
        DMA((n_tp,)),
    ]
    n_attend = len(attend_scratch)

    def kernel(*refs):
        attend_in = refs[:12]
        expert_in = refs[12:18]
        out_ref, settled = refs[18:20]
        own = refs[20:]

        def attention(early):
            attend_kernel(
                early, n_sp, n_tp, nx, kva, kvb, *attend_in, settled, *own[:n_attend]
            )

        expert_kernel(attention, n_sp, n_tp, nx, cap, settled, *expert_in, out_ref, *own[n_attend:])

    return pl.pallas_call(
        kernel,
        out_shape=jax.ShapeDtypeStruct((rows, cols), BF16),
        in_specs=[vm, vm, hbm, hbm, hbm, vm, vm, vm, hbm, hbm, vm, vm, vm, hbm, hbm, hbm, vm, vm],
        out_specs=vm,
        scratch_shapes=[VMEM((rows, cols), BF16)] + attend_scratch + expert_scratch,
        compiler_params=pltpu.CompilerParams(
            collective_id=0, has_side_effects=True, vmem_limit_bytes=60 * 1024 * 1024
        ),
    )(
        query_alpha,
        query_beta,
        pairs_alpha.reshape(rows, -1),
        pairs_beta.reshape(rows, -1),
        off,
        residual_in,
        row(gain_alpha),
        row(gain_beta),
        project_alpha,
        project_beta,
        row(gain_settle),
        row(bias_settle),
        jnp.concatenate([expert_ids.astype(F32), route_weight], axis=1),
        expert_gate,
        expert_up,
        expert_down,
        row(gain_final),
        row(bias_final),
    )


def solution(mesh):
    in_specs = (
        P("sp", "tp"),
        P("sp", "tp"),
        P("sp", "tp", None),
        P("sp", "tp"),
        P("tp"),
        P("sp", "tp"),
        P("sp", "tp", None),
        P("sp", "tp"),
        P("tp"),
        P("tp", None),
        P("tp", None),
        P("tp"),
        P("tp"),
        P("sp", None),
        P("sp", None),
        P("sp", None, "tp"),
        P("sp", None, "tp"),
        P("sp", "tp", None),
        P("tp"),
        P("tp"),
    )
    out_specs = P("sp", "tp")
    return jax.shard_map(body, mesh=mesh, in_specs=in_specs, out_specs=out_specs, check_vma=False)
```

profile of v0, /device:TPU:0, one launch (start us, length us, event | category | flops | bytes accessed | tf_op | source)
XLA Modules:
  0.0 111.0 jit_solution(16420744779430006612)
XLA Ops:
  0.0 0.7 convert_element_type.5
  0.7 0.7 pad_maximum_fusion
  1.4 0.7 maximum_bitcast_fusion
  2.1 0.6 pad.4.refs_4_
  2.7 0.7 copy.23.refs_12_
  3.4 1.6 %copy.27 = bf16[16,8,4,128]{3,1,2,0:T(8,128)(2,1)} copy(bf16[16,8,4,128]{3,2,1,0:T(4,128)(2,1)} %bitcast.17) | data formatting | bytes 262144
  5.0 1.7 %copy.25 = bf16[16,8,4,256]{3,1,2,0:T(8,128)(2,1)} copy(bf16[16,8,4,256]{3,2,1,0:T(4,128)(2,1)} %bitcast.16) | data formatting | bytes 524288
  6.7 102.8 %shard_map.190 = bf16[128,512]{1,0:T(8,128)(2,1)} custom-call(bf16[128,512]{1,0:T(8,128)(2,1)} %refs_0_.1, bf16[128,512]{1,0:T(8,128)(2,1)} %refs_1_.1, bf16[128,512]{1,0:T(8,128)(2,1)} %bitcast.15, bf16[128,1024]{1,0:T(8,128)(2,1)} %bitcast.14, f32[16,128]{1,0:T(8,128)} %pad.4.refs_4_, bf16[128,512]{1,0:T(8,128)(2,1)} %refs_5_.1, f32[1,512]{1,0:T(1,128)} %bitcast.18, ...), custom_call_target="tpu_custom_call" | custom-call | tf_op jit(solution)/shard_map/pallas_call | solution.py:720
  109.5 1.6 %copy.29 = bf16[128,512]{1,0:T(8,128)(2,1)} copy(bf16[128,512]{1,0:T(8,128)(2,1)} %shard_map.190) | data formatting | bytes 262144
where the time goes:
time: 111 us
  Pallas kernels  103 us (93%)
  local copies, waits for them, and re-layouts  6.15 us (6%)
  other arithmetic  2.07 us (2%)
    pallas_call x1, Pallas kernels, body(): pl.pallas_call(kernel, out_shape=jax.ShapeDtypeStruct((rows, cols), BF16)...  103 us
    unnamed x3, local copies, waits for them, and re-layouts  4.82 us

commit v1 on v0

--- a/solution.py
+++ b/solution.py
@@ -327,8 +327,305 @@
     out_ref[...] = norm(first, one, two, gs_ref[...], bs_ref[...], cols * n_tp)
 
 
+def plane_attend(
+    early,
+    n_sp,
+    n_tp,
+    nx,
+    kva,
+    kvb,
+    qa_ref,
+    qb_ref,
+    pairs_a_hbm,
+    pairs_b_hbm,
+    offa_ref,
+    offb_ref,
+    res_ref,
+    ga_ref,
+    gb_ref,
+    pa_hbm,
+    pb_hbm,
+    gs_ref,
+    bs_ref,
+    out_ref,
+    raw_a,
+    raw_b,
+    wide_a,
+    wide_b,
+    own_a,
+    own_b,
+    own_off,
+    qin,
+    kin,
+    oin,
+    keys2,
+    values2,
+    left,
+    acc,
+    obuf,
+    ain,
+    pa,
+    pb,
+    ya,
+    yb,
+    part,
+    got,
+    stat1,
+    stat2,
+    load_sem,
+    in_send,
+    in_recv,
+    o_send,
+    o_recv,
+    part_send,
+    part_recv,
+    s1_send,
+    s1_recv,
+    s2_send,
+    s2_recv,
+):
+    sp = lax.axis_index("sp")
+    tp = lax.axis_index("tp")
+    nz = n_sp // nx
+    z = sp // nx
+    x = lax.rem(sp, nx)
+    rows = qa_ref.shape[0]
+    cols = out_ref.shape[1]
+    tall = nx * rows
+
+    def is_alpha(zz, xx):
+        return lax.rem(zz + xx, 2) == 0
+
+    loads = (
+        pltpu.make_async_copy(pairs_a_hbm, raw_a, load_sem.at[0]),
+        pltpu.make_async_copy(pairs_b_hbm, raw_b, load_sem.at[1]),
+        pltpu.make_async_copy(pa_hbm, pa, load_sem.at[2]),
+        pltpu.make_async_copy(pb_hbm, pb, load_sem.at[3]),
+    )
+    loads[0].start()
+    loads[1].start()
+    for u in range(nz):
+        own_off[u, 0:2] = offa_ref[2 * u : 2 * u + 2]
+        own_off[u, 2:3] = offb_ref[u : u + 1]
+    greet(n_sp, n_tp, sp, tp)
+    loads[0].wait()
+    wide_a[...] = raw_a[...].astype(F32)
+    for u in range(kva):
+        own_a[u] = wide_a[pl.ds(u, rows, stride=kva), :].astype(BF16)
+    loads[1].wait()
+    wide_b[...] = raw_b[...].astype(F32)
+    for u in range(kvb):
+        for h in range(2):
+            own_b[u, h] = wide_b[pl.ds(h * kvb + u, rows, stride=2 * kvb), :].astype(BF16)
+    loads[2].start()
+    loads[3].start()
+
+    def in_copies(zz, xx, alpha):
+        dest = zz * nx + xx
+        where = {"sp": dest, "tp": tp}
+        at = pl.ds(pl.multiple_of(zz * 128, 128), 128)
+        q_ref = qa_ref if alpha else qb_ref
+        kv = (own_a.at[zz], kin.at[0, sp]) if alpha else (own_b.at[zz], kin.at[:, sp])
+        return (
+            remote(own_off.at[zz], oin.at[sp], in_send.at[0, dest], in_recv.at[0, sp], where),
+            remote(q_ref.at[:, at], qin.at[sp], in_send.at[1, dest], in_recv.at[1, sp], where),
+            remote(*kv, in_send.at[2, dest], in_recv.at[2, sp], where),
+        )
+
+    def each_dest(act):
+        def hop(t, carry):
+            away = (t + 1) // 2
+            zz = z + away * (2 * lax.rem(t, 2) - 1)
+            for xx in range(nx):
+                there = (zz >= 0) & (zz < nz) & ((zz != z) | (xx != x))
+                for alpha in (True, False):
+
+                    @pl.when(there & (is_alpha(zz, xx) == alpha))
+                    def _(xx=xx, alpha=alpha):
+                        for copy in in_copies(zz, xx, alpha):
+                            act(copy)
+
+            return carry
+
+        lax.fori_loop(0, 2 * nz - 1, hop, 0)
+
+    each_dest(lambda copy: copy.start())
+    early()
+
+    def o_copy(d):
+        return remote(obuf.at[d], ain.at[sp], o_send.at[d], o_recv.at[sp], {"sp": d, "tp": tp})
+
+    lane_t = lax.broadcasted_iota(jnp.int32, (tall, tall), 1)
+    row_t = lax.broadcasted_iota(jnp.int32, (tall, tall), 0)
+    lane = lax.broadcasted_iota(jnp.int32, (tall, 128), 1)
+    tri = jnp.where(row_t > lane_t, 1.0, 0.0).astype(BF16)
+
+    def attend(alpha):
+        heads = 2 if alpha else 1
+        scale = 64**-0.5 if alpha else 128**-0.5
+        at = pl.ds(pl.multiple_of(z * 128, 128), 128)
+        oin[sp] = own_off[z]
+        if alpha:
+            qin[sp] = qa_ref[:, at]
+            kin[0, sp] = own_a[z]
+        else:
+            qin[sp] = qb_ref[:, at]
+            kin[:, sp] = own_b[z]
+
+        def arrive(p):
+            for xx in range(nx):
+                s = p * nx + xx
+
+                @pl.when(s != sp)
+                def _(s=s):
+                    where = {"sp": sp, "tp": tp}
+                    kv = kin.at[0, s] if alpha else kin.at[:, s]
+                    remote(oin.at[s], oin.at[s], in_send.at[0, 0], in_recv.at[0, s], where).wait_recv()
+                    remote(qin.at[s], qin.at[s], in_send.at[1, 0], in_recv.at[1, s], where).wait_recv()
+                    remote(kv, kv, in_send.at[2, 0], in_recv.at[2, s], where).wait_recv()
+
+            if alpha:
+                pair = kin[0, pl.ds(p * nx, nx)].reshape(tall, 128).astype(F32)
+                turned = pltpu.roll(pair, 64, 1)
+                keys2[p, 0:tall] = jnp.where(lane < 64, pair, 0.0).astype(BF16)
+                keys2[p, tall:] = jnp.where(lane < 64, 0.0, turned).astype(BF16)
+                values2[p, 0:tall] = jnp.where(lane < 64, turned, 0.0).astype(BF16)
+                values2[p, tall:] = jnp.where(lane < 64, 0.0, pair).astype(BF16)
+
+        def step(r, c, diag):
+            query = qin[pl.ds(r * nx, nx)].reshape(tall, 128)
+            if alpha:
+                key, value = keys2[c], values2[c]
+            else:
+                key = kin[0, pl.ds(c * nx, nx)].reshape(tall, 128)
+                value = kin[1, pl.ds(c * nx, nx)].reshape(tall, 128)
+            scores = lax.dot_general(query, key, (((1,), (1,)), ((), ())), preferred_element_type=F32)
+            valid = lane_t < row_t
+            ws = []
+            for h in range(heads):
+                row = h if alpha else 2
+                offset = jnp.concatenate([oin[c * nx + i, row : row + 1, :] for i in range(nx)], axis=1)
+                s = scores[:, h * tall : (h + 1) * tall] * scale + offset
+                soft = jnp.maximum(s, 0.0) + jnp.log(1.0 + jnp.exp(-jnp.abs(s)))
+                used = jnp.where(valid, soft, 0.0) if diag else soft
+                sums = jnp.dot(used.astype(BF16), tri, preferred_element_type=F32)
+                total = jnp.broadcast_to(sums[:, 0:1] + used[:, 0:1], (tall, 128))
+                e = s - soft - sums
+                if diag:
+                    w = jnp.where(valid, jnp.exp(e), 0.0)
+                    left[h, r] = -total
+                else:
+                    before = left[h, r]
+                    w = jnp.exp(e + jnp.concatenate([before] * nx, axis=1))
+                    left[h, r] = before - total
+                ws.append(w.astype(BF16))
+            w = ws[0] if heads == 1 else jnp.concatenate(ws, axis=1)
+            o = jnp.dot(w, value, preferred_element_type=F32)
+            o = o if diag else acc[r] + o
+            acc[r] = o
+
+            @pl.when(c == 0)
+            def _():
+                obuf[pl.ds(r * nx, nx)] = o.astype(BF16).reshape(nx, rows, 128)
+                for xx in range(nx):
+                    d = r * nx + xx
+
+                    @pl.when(d != sp)
+                    def _(d=d):
+                        o_copy(d).start()
+
+                    @pl.when(d == sp)
+                    def _(d=d):
+                        ain[sp] = obuf[d]
+
+        def phase(k, span):
+            low, high = span
+            lower_half = z < nz // 2
+            up = jnp.where(lower_half, low == 0, high < nz - 1).astype(jnp.int32)
+            first = (k == 0).astype(jnp.int32)
+            p = first * z + (1 - first) * (up * (high + 1) + (1 - up) * (low - 1))
+            arrive(p)
+            step(p, p, True)
+            count = (1 - first) * (high - low + 1)
+
+            def more(t, carry):
+                step(p + t * (1 - up), p - t * up, False)
+                return carry
+
+            lax.fori_loop(1, count + 1, more, 0)
+            return jnp.minimum(low, p), jnp.maximum(high, p)
+
+        lax.fori_loop(0, nz, phase, (z, z))
+
+    for alpha in (True, False):
+
+        @pl.when(is_alpha(z, x) == alpha)
+        def _(alpha=alpha):
+            attend(alpha)
+
+    def o_wait(j, carry):
+        @pl.when(j != sp)
+        def _():
+            remote(obuf.at[j], ain.at[j], o_send.at[0], o_recv.at[j], {"sp": sp, "tp": tp}).wait_recv()
+
+        return carry
+
+    lax.fori_loop(0, n_sp, o_wait, 0)
+    wide = kva * 128
+    aa = jnp.concatenate([ain[k * nx + k % 2] for k in range(nz)], axis=1).astype(F32)
+    ab = jnp.concatenate([ain[k * nx + 1 - k % 2] for k in range(nz)], axis=1).astype(F32)
+    stats_start(n_tp, sp, tp, lane_sums(aa * aa), lane_sums(ab * ab), stat1, s1_send, s1_recv)
+    loads[2].wait()
+    loads[3].wait()
+    na = (aa * ga_ref[...]).astype(BF16)
+    nb = (ab * gb_ref[...]).astype(BF16)
+    for t in range(n_tp):
+        ya[t] = jnp.dot(na, pa[:, t * cols : (t + 1) * cols], preferred_element_type=F32)
+        yb[t] = jnp.dot(nb, pb[:, t * cols : (t + 1) * cols], preferred_element_type=F32)
+    sq_a, sq_b = stats_finish(n_tp, sp, tp, stat1, s1_send, s1_recv, rows)
+    scale_a = lax.rsqrt(sq_a / (wide * n_tp) + norm_eps)
+    scale_b = lax.rsqrt(sq_b / (kvb * 128 * n_tp) + norm_eps)
+
+    def part_copy(o):
+        peer = lax.rem(tp + o, n_tp)
+        return remote(
+            part.at[peer], got.at[tp], part_send.at[o], part_recv.at[tp], {"sp": sp, "tp": peer}
+        )
+
+    for o in range(1, n_tp):
+        peer = lax.rem(tp + o, n_tp)
+        part[peer] = (ya[peer] * scale_a + yb[peer] * scale_b).astype(BF16)
+        part_copy(o).start()
+    total = (ya[tp] * scale_a + yb[tp] * scale_b).astype(BF16).astype(F32)
+    for o in range(1, n_tp):
+        peer = lax.rem(tp + o, n_tp)
+        remote(
+            part.at[peer], got.at[peer], part_send.at[o], part_recv.at[peer], {"sp": sp, "tp": peer}
+        ).wait_recv()
+        total = total + got[peer].astype(F32)
+    mixed = total.astype(BF16).astype(F32)
+    first = depth_scale * res_ref[...].astype(F32) + mixed
+    stats_start(n_tp, sp, tp, lane_sums(first), lane_sums(first * first), stat2, s2_send, s2_recv)
+    for o in range(1, n_tp):
+        part_copy(o).wait_send()
+
+    each_dest(lambda copy: copy.wait_send())
+
+    def o_drain(j, carry):
+        @pl.when(j != sp)
+        def _():
+            o_copy(j).wait_send()
+
+        return carry
+
+    lax.fori_loop(0, n_sp, o_drain, 0)
+    one, two = stats_finish(n_tp, sp, tp, stat2, s2_send, s2_recv, rows)
+    out_ref[...] = norm(first, one, two, gs_ref[...], bs_ref[...], cols * n_tp)
+
+
 def expert_kernel(
     attention,
+    balanced,
     n_sp,
     n_tp,
     nx,
@@ -414,11 +711,17 @@
         for copy in x_copies(j):
             copy.start()
 
-    ahead = jnp.maximum(sp // nx - 1, 0) * nx
-
-    for load in loads:
-        load.start()
-    attention(lambda: loop(0, ahead, spread_out))
+    ahead = 0 if balanced else jnp.maximum(sp // nx - 1, 0) * nx
+
+    def start_loads():
+        for load in loads:
+            load.start()
+
+    if balanced:
+        attention(start_loads)
+    else:
+        start_loads()
+        attention(lambda: loop(0, ahead, spread_out))
     ids = ids_ref[...][:, 0:2]
     expert = lax.broadcasted_iota(jnp.int32, (rows, 128), 1).astype(F32)
     hot = [jnp.where(ids[:, k : k + 1] == expert, 1.0, 0.0) for k in range(2)]
@@ -632,8 +935,6 @@
     kvb = pairs_beta.shape[1]
     heads = 2 * kva + kvb
     heads_pad = -(-heads // 8) * 8
-    off = jnp.transpose(jnp.concatenate([offset_alpha, offset_beta], axis=1))
-    off = jnp.pad(off, ((0, heads_pad - heads), (0, 0)))
     kv_cols = kva * 128 + kvb * 256
     inner = kva * 128
     inner_b = kvb * 128
@@ -670,6 +971,47 @@
         DMA((n_tp,)),
         DMA((n_tp,)),
     ]
+    balanced = nx == 2 and kva == nz and kvb == nz
+    tall = nx * rows
+    plane_scratch = [
+        VMEM((rows * kva, 128), BF16),
+        VMEM((rows * kvb * 2, 128), BF16),
+        VMEM((rows * kva, 128), F32),
+        VMEM((rows * kvb * 2, 128), F32),
+        VMEM((kva, rows, 128), BF16),
+        VMEM((kvb, 2, rows, 128), BF16),
+        VMEM((nz, 8, 128), F32),
+        VMEM((n_sp, rows, 128), BF16),
+        VMEM((2, n_sp, rows, 128), BF16),
+        VMEM((n_sp, 8, 128), F32),
+        VMEM((nz, 2 * tall, 128), BF16),
+        VMEM((nz, 2 * tall, 128), BF16),
+        VMEM((2, nz, tall, 128), F32),
+        VMEM((nz, tall, 128), F32),
+        VMEM((n_sp, rows, 128), BF16),
+        VMEM((n_sp, rows, 128), BF16),
+        VMEM(project_alpha.shape, BF16),
+        VMEM(project_beta.shape, BF16),
+        VMEM((n_tp, rows, cols), F32),
+        VMEM((n_tp, rows, cols), F32),
+        VMEM((n_tp, rows, cols), BF16),
+        VMEM((n_tp, rows, cols), BF16),
+        VMEM((n_tp, 2, 8, rows), F32),
+        VMEM((n_tp, 2, 8, rows), F32),
+        DMA((4,)),
+        DMA((3, n_sp)),
+        DMA((3, n_sp)),
+        DMA((n_sp,)),
+        DMA((n_sp,)),
+        DMA((n_tp,)),
+        DMA((n_tp,)),
+        DMA((n_tp,)),
+        DMA((n_tp,)),
+        DMA((n_tp,)),
+        DMA((n_tp,)),
+    ]
+    if balanced:
+        attend_scratch = plane_scratch
     expert_scratch = [
         VMEM((width, units), BF16),
         VMEM((width, units), BF16),
@@ -703,24 +1045,38 @@
         DMA((n_tp,)),
     ]
     n_attend = len(attend_scratch)
+    if balanced:
+        halves = pairs_beta.reshape(rows, kvb, 2, 128).transpose(0, 2, 1, 3)
+        keyed = [
+            pairs_alpha.reshape(rows * kva, 128),
+            halves.reshape(rows * kvb * 2, 128),
+            offset_alpha.T,
+            offset_beta.T,
+        ]
+        places_in = [vm, vm]
+    else:
+        off = jnp.transpose(jnp.concatenate([offset_alpha, offset_beta], axis=1))
+        off = jnp.pad(off, ((0, heads_pad - heads), (0, 0)))
+        keyed = [pairs_alpha.reshape(rows, -1), pairs_beta.reshape(rows, -1), off]
+        places_in = [hbm]
+    n_in = len(keyed) + 9
 
     def kernel(*refs):
-        attend_in = refs[:12]
-        expert_in = refs[12:18]
-        out_ref, settled = refs[18:20]
-        own = refs[20:]
+        attend_in = refs[:n_in]
+        expert_in = refs[n_in : n_in + 6]
+        out_ref, settled = refs[n_in + 6 : n_in + 8]
+        own = refs[n_in + 8 :]
 
         def attention(early):
-            attend_kernel(
-                early, n_sp, n_tp, nx, kva, kvb, *attend_in, settled, *own[:n_attend]
-            )
-
-        expert_kernel(attention, n_sp, n_tp, nx, cap, settled, *expert_in, out_ref, *own[n_attend:])
+            attend = plane_attend if balanced else attend_kernel
+            attend(early, n_sp, n_tp, nx, kva, kvb, *attend_in, settled, *own[:n_attend])
+
+        expert_kernel(attention, balanced, n_sp, n_tp, nx, cap, settled, *expert_in, out_ref, *own[n_attend:])
 
     return pl.pallas_call(
         kernel,
         out_shape=jax.ShapeDtypeStruct((rows, cols), BF16),
-        in_specs=[vm, vm, hbm, hbm, hbm, vm, vm, vm, hbm, hbm, vm, vm, vm, hbm, hbm, hbm, vm, vm],
+        in_specs=[vm, vm, hbm, hbm] + places_in + [vm, vm, vm, hbm, hbm, vm, vm, vm, hbm, hbm, hbm, vm, vm],
         out_specs=vm,
         scratch_shapes=[VMEM((rows, cols), BF16)] + attend_scratch + expert_scratch,
         compiler_params=pltpu.CompilerParams(
@@ -729,9 +1085,7 @@
     )(
         query_alpha,
         query_beta,
-        pairs_alpha.reshape(rows, -1),
-        pairs_beta.reshape(rows, -1),
-        off,
+        *keyed,
         residual_in,
         row(gain_alpha),
         row(gain_beta),

time: 111 us -> 90.7 us (0.82)
  Pallas kernels: 103 us -> 86.8 us
  local copies, waits for them, and re-layouts: 6.15 us -> 2.31 us
    pallas_call x1, Pallas kernels: 103 us -> 86.8 us  [body(): pl.pallas_call(kernel, out_shape=jax.ShapeDtypeStruct((rows, cols), BF16)...]
    unnamed x3 -> x1, local copies, waits for them, and re-layouts: 4.82 us -> 1.57 us
where the time goes in v1:
time: 90.7 us; the launch traced here: 90.5 us
  Pallas kernels  86.8 us (96%)
  local copies, waits for them, and re-layouts  2.31 us (3%)
  other arithmetic  1.37 us (2%)
    pallas_call x1, Pallas kernels, body(): pl.pallas_call(kernel, out_shape=jax.ShapeDtypeStruct((rows, cols), BF16)...  86.8 us

profile of v1, /device:TPU:0, one launch (start us, length us, event | category | flops | bytes accessed | tf_op | source)
XLA Modules:
  0.0 90.5 jit_solution(8662022729414198226)
XLA Ops:
  0.0 0.7 convert_element_type.3
  0.7 0.7 pad_maximum_fusion
  1.4 0.7 copy.25.refs_13_
  2.1 86.8 %shard_map.190 = bf16[128,512]{1,0:T(8,128)(2,1)} custom-call(bf16[128,512]{1,0:T(8,128)(2,1)} %refs_0_.1, bf16[128,512]{1,0:T(8,128)(2,1)} %refs_1_.1, bf16[512,128]{1,0:T(8,128)(2,1)} %bitcast.15, bf16[1024,128]{1,0:T(8,128)(2,1)} %bitcast.14, f32[8,128]{1,0:T(8,128)} %bitcast.16, f32[4,128]{1,0:T(4,128)} %bitcast.17, bf16[128,512]{1,0:T(8,128)(2,1)} %refs_6_.1, ...), custom_call_target="tpu_custom_call" | custom-call | tf_op jit(solution)/shard_map/pallas_call | solution.py:1076
  88.9 1.6 %copy.27 = bf16[128,512]{1,0:T(8,128)(2,1)} copy(bf16[128,512]{1,0:T(8,128)(2,1)} %shard_map.190) | data formatting | bytes 262144

commit v2 on v1

--- a/solution.py
+++ b/solution.py
@@ -329,6 +329,7 @@
 
 def plane_attend(
     early,
+    between,
     n_sp,
     n_tp,
     nx,
@@ -563,6 +564,8 @@
         def _(alpha=alpha):
             attend(alpha)
 
+    between()
+
     def o_wait(j, carry):
         @pl.when(j != sp)
         def _():
@@ -625,7 +628,6 @@
 
 def expert_kernel(
     attention,
-    balanced,
     n_sp,
     n_tp,
     nx,
@@ -711,17 +713,11 @@
         for copy in x_copies(j):
             copy.start()
 
-    ahead = 0 if balanced else jnp.maximum(sp // nx - 1, 0) * nx
-
-    def start_loads():
-        for load in loads:
-            load.start()
-
-    if balanced:
-        attention(start_loads)
-    else:
-        start_loads()
-        attention(lambda: loop(0, ahead, spread_out))
+    ahead = jnp.maximum(sp // nx - 1, 0) * nx
+
+    for load in loads:
+        load.start()
+    attention(lambda: loop(0, ahead, spread_out))
     ids = ids_ref[...][:, 0:2]
     expert = lax.broadcasted_iota(jnp.int32, (rows, 128), 1).astype(F32)
     hot = [jnp.where(ids[:, k : k + 1] == expert, 1.0, 0.0) for k in range(2)]
@@ -900,6 +896,354 @@
     loop(1, n_sp, drain_sp)
     for k in range(ny):
         d_copy(k).wait_send()
+    one, two = stats_finish(n_tp, sp, tp, stat, s_send, s_recv, rows)
+    out_ref[...] = norm(second, one, two, gf_ref[...], bf_ref[...], cols * n_tp)
+
+
+def plane_expert(
+    attention,
+    n_sp,
+    n_tp,
+    nx,
+    cap,
+    set_ref,
+    ids_ref,
+    weight_ref,
+    wg_hbm,
+    wu_hbm,
+    wd_hbm,
+    gf_ref,
+    bf_ref,
+    out_ref,
+    wg,
+    wu,
+    wd,
+    hits,
+    wpack,
+    wrecv,
+    wcol,
+    packed,
+    xbuf,
+    gate,
+    up,
+    hid,
+    away,
+    arrived,
+    home,
+    mid,
+    midx,
+    midy,
+    gotd,
+    gotx,
+    goty,
+    outb,
+    back,
+    stat,
+    load_sem,
+    w_send,
+    w_recv,
+    a_send,
+    a_recv,
+    x_send,
+    x_recv,
+    d_send,
+    d_recv,
+    m_send,
+    m_recv,
+    b_send,
+    b_recv,
+    s_send,
+    s_recv,
+):
+    sp = lax.axis_index("sp")
+    tp = lax.axis_index("tp")
+    rows, cols = set_ref.shape
+    nz = n_sp // nx
+    z = sp // nx
+    x = lax.rem(sp, nx)
+    core = lax.rem(tp, 2)
+    y = tp // 2
+    mate = y * 2 + 1 - core
+    far = (1 - y) * 2 + core
+    far_mate = (1 - y) * 2 + 1 - core
+    to_mate = {"sp": sp, "tp": mate}
+    to_x = {"sp": z * nx + 1 - x, "tp": tp}
+    to_y = {"sp": sp, "tp": far}
+    table = [sorted(range(nz), key=lambda g: (abs(g - a), (g - a) * (1 if a < nz // 2 else -1))) for a in range(nz)]
+
+    def near(i):
+        pick = table[0][i]
+        for a in range(1, nz):
+            pick = jnp.where(z == a, table[a][i], pick)
+        return pick
+
+    loads = (
+        pltpu.make_async_copy(wg_hbm.at[0], wg, load_sem.at[0]),
+        pltpu.make_async_copy(wu_hbm.at[0], wu, load_sem.at[1]),
+        pltpu.make_async_copy(wd_hbm.at[0], wd, load_sem.at[2]),
+    )
+
+    def w_copy(d):
+        return remote(wpack.at[d // nx], wrecv.at[sp], w_send.at[d], w_recv.at[sp], {"sp": d, "tp": tp})
+
+    def others(fn):
+        def one(d, carry):
+            @pl.when(d != sp)
+            def _():
+                fn(d)
+
+            return carry
+
+        lax.fori_loop(0, n_sp, one, 0)
+
+    def early():
+        for load in loads:
+            load.start()
+        ids = [ids_ref[k : k + 1, :] for k in range(2)]
+        r = lax.broadcasted_iota(jnp.int32, (rows, rows), 0)
+        c = lax.broadcasted_iota(jnp.int32, (rows, rows), 1)
+        upper = jnp.where(r < c, 1.0, 0.0).astype(BF16)
+        group = lax.broadcasted_iota(jnp.int32, (8, rows), 0) * nx
+        hot = jnp.where((ids[0] >= group) & (ids[0] < group + nx), 1.0, 0.0)
+        before = jnp.dot(hot.astype(BF16), upper, preferred_element_type=F32)
+        seat = lax.broadcasted_iota(jnp.int32, (cap, rows), 0).astype(F32)
+        for g in range(nz):
+            match = jnp.where(seat == before[g : g + 1], hot[g : g + 1], 0.0).astype(BF16)
+            hits[g * cap : (g + 1) * cap] = match
+            share = [
+                jnp.where(ids[0] == g * nx + e, weight_ref[0:1, :], 0.0)
+                + jnp.where(ids[1] == g * nx + e, weight_ref[1:2, :], 0.0)
+                for e in range(nx)
+            ]
+            line = lax.broadcasted_iota(jnp.int32, (8, rows), 0)
+            both = jnp.where(line == 0, share[0], jnp.where(line == 1, share[1], 0.0))
+            high, low = split(both)
+            dims = (((1,), (1,)), ((), ()))
+            wpack[g] = jnp.zeros((8, 128), F32)
+            wpack[g, :, 0:cap] = lax.dot_general(high, match, dims, preferred_element_type=F32) + lax.dot_general(
+                low, match, dims, preferred_element_type=F32
+            )
+        others(lambda d: w_copy(d).start())
+        wrecv[sp] = wpack[z]
+
+    def between():
+        def spread(j, carry):
+            @pl.when(j != sp)
+            def _():
+                remote(wrecv.at[j], wrecv.at[j], w_send.at[0], w_recv.at[j], {"sp": sp, "tp": tp}).wait_recv()
+
+            wide = jnp.transpose(jnp.broadcast_to(wrecv[j, pl.ds(x, 1), :], (128, 128)))
+            wcol[lax.rem(j, nx), j // nx] = wide[0:cap]
+            return carry
+
+        lax.fori_loop(0, n_sp, spread, 0)
+
+    attention(early, between)
+
+    sent = jnp.dot(hits[...], set_ref[...], preferred_element_type=F32).astype(BF16)
+    packed[...] = sent.reshape(nz, cap, cols)
+
+    def a_copy(i):
+        g = near(i)
+        return remote(packed.at[g], xbuf.at[tp, x, z], a_send.at[i], a_recv.at[z], {"sp": g * nx + x, "tp": tp})
+
+    for i in range(1, nz):
+        a_copy(i).start()
+    xbuf[tp, x, z] = packed[z]
+
+    def x_copy(kind, t, xs, g, where):
+        block = xbuf.at[t, xs, g]
+        return remote(block, block, x_send.at[kind, g], x_recv.at[t, xs, g], where)
+
+    def x_wait(t, xs, g):
+        block = xbuf.at[t, xs, g]
+        remote(block, block, x_send.at[0, 0], x_recv.at[t, xs, g], to_mate).wait_recv()
+
+    def when_x_first(g, fn):
+        pl.when(lax.rem(g, 2) == 0)(fn)
+
+    def when_y_first(g, fn):
+        pl.when(lax.rem(g, 2) == 1)(fn)
+
+    def own_out(i):
+        g = near(i)
+        if i:
+            remote(packed.at[g], xbuf.at[tp, x, g], a_send.at[0], a_recv.at[g], to_mate).wait_recv()
+        x_copy(1, tp, x, g, to_x).start()
+        x_copy(2, tp, x, g, to_y).start()
+        x_copy(0, tp, x, g, to_mate).start()
+
+    def pass_on(i):
+        g = near(i)
+        x_wait(tp, 1 - x, g)
+        when_x_first(g, lambda: x_copy(4, tp, 1 - x, g, to_y).start())
+        x_copy(3, tp, 1 - x, g, to_mate).start()
+        x_wait(far, x, g)
+        when_y_first(g, lambda: x_copy(6, far, x, g, to_x).start())
+        x_copy(5, far, x, g, to_mate).start()
+
+    def pass_diag(i):
+        g = near(i)
+        x_wait(far, 1 - x, g)
+        x_copy(7, far, 1 - x, g, to_mate).start()
+
+    def piece(t, xs, fresh):
+        block = xbuf[t, xs].reshape(nz * cap, cols)
+        at = pl.ds(pl.multiple_of(t * cols, 128), cols)
+        g = jnp.dot(block, wg[at, :], preferred_element_type=F32)
+        u = jnp.dot(block, wu[at, :], preferred_element_type=F32)
+        if fresh:
+            gate[xs] = g
+            up[xs] = u
+        else:
+            gate[xs] += g
+            up[xs] += u
+
+    def all_in(t, xs):
+        def one(g, carry):
+            x_wait(t, xs, g)
+            return carry
+
+        lax.fori_loop(0, nz, one, 0)
+
+    for i in range(nz + 2):
+        if i < nz:
+            own_out(i)
+        if 1 <= i <= nz:
+            pass_on(i - 1)
+        if i >= 2:
+            pass_diag(i - 2)
+        if i == nz - 1:
+            loads[0].wait()
+            loads[1].wait()
+            piece(tp, x, True)
+        if i == nz:
+            all_in(mate, x)
+            piece(mate, x, False)
+            piece(tp, 1 - x, True)
+    piece(far, x, False)
+    all_in(far_mate, x)
+    piece(far_mate, x, False)
+    all_in(mate, 1 - x)
+    piece(mate, 1 - x, False)
+    piece(far, 1 - x, False)
+    all_in(far_mate, 1 - x)
+    piece(far_mate, 1 - x, False)
+    for xs in range(nx):
+        value = gate[xs]
+        weight = jnp.concatenate([wcol[xs].reshape(nz * cap, 128)] * (value.shape[1] // 128), axis=1)
+        hid[xs * nz * cap : (xs + 1) * nz * cap] = (value / (1.0 + jnp.exp(-value)) * up[xs] * weight).astype(BF16)
+    loads[2].wait()
+
+    def down(t):
+        at = pl.ds(pl.multiple_of(t * cols, 128), cols)
+        result = jnp.dot(hid[...], wd[:, at], preferred_element_type=F32)
+        return result.astype(BF16).reshape(nx, nz, cap, cols)
+
+    def d_copy(k, xs):
+        return remote(away.at[k, xs], arrived.at[k, xs], d_send.at[k, xs], d_recv.at[k, xs], to_mate)
+
+    away[1] = down(far_mate)
+    d_copy(1, 1 - x).start()
+    d_copy(1, x).start()
+    away[0] = down(mate)
+    d_copy(0, 1 - x).start()
+    d_copy(0, x).start()
+    home[1] = down(far)
+
+    def pair(k, xs, g):
+        return home[k, xs, g].astype(F32) + arrived[k, xs, g].astype(F32)
+
+    def m_copy(kind, src, dst, g, where):
+        return remote(src.at[g], dst.at[g], m_send.at[kind, g], m_recv.at[kind, g], where)
+
+    def diag_copy(g, where):
+        return m_copy(0, mid, gotd, g, where)
+
+    def x_send_copy(g):
+        return m_copy(1, midx, gotx, g, to_x)
+
+    def y_send_copy(g):
+        return m_copy(2, midy, goty, g, to_y)
+
+    order = range(nz - 1, -1, -1)
+    d_copy(1, 1 - x).wait_recv()
+    for i in order:
+        g = near(i)
+        mid[g] = pair(1, 1 - x, g).astype(BF16)
+        when_x_first(g, lambda g=g: diag_copy(g, to_x).start())
+        when_y_first(g, lambda g=g: diag_copy(g, to_y).start())
+    home[0] = down(tp)
+    d_copy(1, x).wait_recv()
+    d_copy(0, 1 - x).wait_recv()
+    for i in order:
+        g = near(i)
+
+        def plain_x(g=g):
+            midx[g] = pair(0, 1 - x, g).astype(BF16)
+            x_send_copy(g).start()
+
+        def plain_y(g=g):
+            midy[g] = pair(1, x, g).astype(BF16)
+            y_send_copy(g).start()
+
+        when_x_first(g, plain_x)
+        when_y_first(g, plain_y)
+    for i in order:
+        g = near(i)
+        diag_copy(g, to_mate).wait_recv()
+
+        def joined_y(g=g):
+            midy[g] = (pair(1, x, g) + gotd[g].astype(F32)).astype(BF16)
+            y_send_copy(g).start()
+
+        def joined_x(g=g):
+            midx[g] = (pair(0, 1 - x, g) + gotd[g].astype(F32)).astype(BF16)
+            x_send_copy(g).start()
+
+        when_x_first(g, joined_y)
+        when_y_first(g, joined_x)
+
+    def b_copy(i):
+        g = near(i)
+        return remote(outb.at[g], back.at[z], b_send.at[i], b_recv.at[z], {"sp": g * nx + x, "tp": tp})
+
+    d_copy(0, x).wait_recv()
+    for i in order:
+        g = near(i)
+        x_send_copy(g).wait_recv()
+        y_send_copy(g).wait_recv()
+        total = (pair(0, x, g) + gotx[g].astype(F32) + goty[g].astype(F32)).astype(BF16)
+        if i:
+            outb[g] = total
+            b_copy(i).start()
+        else:
+            back[z] = total
+    for i in range(1, nz):
+        g = near(i)
+        remote(outb.at[g], back.at[g], b_send.at[0], b_recv.at[g], to_mate).wait_recv()
+    flat = back[...].reshape(nz * cap, cols)
+    routed = lax.dot_general(hits[...], flat, (((0,), (0,)), ((), ())), preferred_element_type=F32)
+    second = depth_scale * set_ref[...].astype(F32) + routed
+    stats_start(n_tp, sp, tp, lane_sums(second), lane_sums(second * second), stat, s_send, s_recv)
+    others(lambda d: w_copy(d).wait_send())
+    for i in range(nz):
+        g = near(i)
+        if i:
+            a_copy(i).wait_send()
+            b_copy(i).wait_send()
+        x_copy(1, tp, x, g, to_x).wait_send()
+        x_copy(2, tp, x, g, to_y).wait_send()
+        for kind in (0, 3, 5, 7):
+            x_copy(kind, tp, x, g, to_mate).wait_send()
+        when_x_first(g, lambda g=g: x_copy(4, tp, 1 - x, g, to_y).wait_send())
+        when_y_first(g, lambda g=g: x_copy(6, far, x, g, to_x).wait_send())
+        diag_copy(g, to_mate).wait_send()
+        x_send_copy(g).wait_send()
+        y_send_copy(g).wait_send()
+    for k in range(2):
+        d_copy(k, 0).wait_send()
+        d_copy(k, 1).wait_send()
     one, two = stats_finish(n_tp, sp, tp, stat, s_send, s_recv, rows)
     out_ref[...] = norm(second, one, two, gf_ref[...], bf_ref[...], cols * n_tp)
 
@@ -971,7 +1315,7 @@
         DMA((n_tp,)),
         DMA((n_tp,)),
     ]
-    balanced = nx == 2 and kva == nz and kvb == nz
+    balanced = nx == 2 and ny == 2 and kva == nz and kvb == nz and cap % 16 == 0
     tall = nx * rows
     plane_scratch = [
         VMEM((rows * kva, 128), BF16),
@@ -1010,8 +1354,6 @@
         DMA((n_tp,)),
         DMA((n_tp,)),
     ]
-    if balanced:
-        attend_scratch = plane_scratch
     expert_scratch = [
         VMEM((width, units), BF16),
         VMEM((width, units), BF16),
@@ -1044,6 +1386,50 @@
         DMA((n_tp,)),
         DMA((n_tp,)),
     ]
+    block = (nz, cap, cols)
+    grouped_scratch = [
+        VMEM((width, units), BF16),
+        VMEM((width, units), BF16),
+        VMEM((units, width), BF16),
+        VMEM((nz * cap, rows), BF16),
+        VMEM((nz, 8, 128), F32),
+        VMEM((n_sp, 8, 128), F32),
+        VMEM((nx, nz, cap, 128), F32),
+        VMEM(block, BF16),
+        VMEM((n_tp, nx) + block, BF16),
+        VMEM((nx, nz * cap, units), F32),
+        VMEM((nx, nz * cap, units), F32),
+        VMEM((places, units), BF16),
+        VMEM((ny, nx) + block, BF16),
+        VMEM((ny, nx) + block, BF16),
+        VMEM((ny, nx) + block, BF16),
+        VMEM(block, BF16),
+        VMEM(block, BF16),
+        VMEM(block, BF16),
+        VMEM(block, BF16),
+        VMEM(block, BF16),
+        VMEM(block, BF16),
+        VMEM(block, BF16),
+        VMEM(block, BF16),
+        VMEM((n_tp, 2, 8, rows), F32),
+        DMA((3,)),
+        DMA((n_sp,)),
+        DMA((n_sp,)),
+        DMA((nz,)),
+        DMA((nz,)),
+        DMA((8, nz)),
+        DMA((n_tp, nx, nz)),
+        DMA((ny, nx)),
+        DMA((ny, nx)),
+        DMA((3, nz)),
+        DMA((3, nz)),
+        DMA((nz,)),
+        DMA((nz,)),
+        DMA((n_tp,)),
+        DMA((n_tp,)),
+    ]
+    if balanced:
+        attend_scratch, expert_scratch = plane_scratch, grouped_scratch
     n_attend = len(attend_scratch)
     if balanced:
         halves = pairs_beta.reshape(rows, kvb, 2, 128).transpose(0, 2, 1, 3)
@@ -1054,29 +1440,33 @@
             offset_beta.T,
         ]
         places_in = [vm, vm]
+        routes = [expert_ids.T, route_weight.T]
     else:
         off = jnp.transpose(jnp.concatenate([offset_alpha, offset_beta], axis=1))
         off = jnp.pad(off, ((0, heads_pad - heads), (0, 0)))
         keyed = [pairs_alpha.reshape(rows, -1), pairs_beta.reshape(rows, -1), off]
         places_in = [hbm]
+        routes = [jnp.concatenate([expert_ids.astype(F32), route_weight], axis=1)]
     n_in = len(keyed) + 9
+    n_all = n_in + len(routes) + 5
 
     def kernel(*refs):
         attend_in = refs[:n_in]
-        expert_in = refs[n_in : n_in + 6]
-        out_ref, settled = refs[n_in + 6 : n_in + 8]
-        own = refs[n_in + 8 :]
-
-        def attention(early):
+        out_ref, settled = refs[n_all : n_all + 2]
+        expert_in = refs[n_in:n_all]
+        own = refs[n_all + 2 :]
+
+        def attention(*hooks):
             attend = plane_attend if balanced else attend_kernel
-            attend(early, n_sp, n_tp, nx, kva, kvb, *attend_in, settled, *own[:n_attend])
-
-        expert_kernel(attention, balanced, n_sp, n_tp, nx, cap, settled, *expert_in, out_ref, *own[n_attend:])
+            attend(*hooks, n_sp, n_tp, nx, kva, kvb, *attend_in, settled, *own[:n_attend])
+
+        expert = plane_expert if balanced else expert_kernel
+        expert(attention, n_sp, n_tp, nx, cap, settled, *expert_in, out_ref, *own[n_attend:])
 
     return pl.pallas_call(
         kernel,
         out_shape=jax.ShapeDtypeStruct((rows, cols), BF16),
-        in_specs=[vm, vm, hbm, hbm] + places_in + [vm, vm, vm, hbm, hbm, vm, vm, vm, hbm, hbm, hbm, vm, vm],
+        in_specs=[vm, vm, hbm, hbm] + places_in + [vm] * 3 + [hbm] * 2 + [vm] * (2 + len(routes)) + [hbm] * 3 + [vm] * 2,
         out_specs=vm,
         scratch_shapes=[VMEM((rows, cols), BF16)] + attend_scratch + expert_scratch,
         compiler_params=pltpu.CompilerParams(
@@ -1093,7 +1483,7 @@
         project_beta,
         row(gain_settle),
         row(bias_settle),
-        jnp.concatenate([expert_ids.astype(F32), route_weight], axis=1),
+        *routes,
         expert_gate,
         expert_up,
         expert_down,

time: 90.7 us -> 86.2 us (0.950)
  Pallas kernels: 86.8 us -> 84.5 us
  other arithmetic: 1.37 us -> 0 us
    pallas_call x1, Pallas kernels: 86.8 us -> 84.5 us  [body(): pl.pallas_call(kernel, out_shape=jax.ShapeDtypeStruct((rows, cols), BF16)...]
where the time goes in v2:
time: 86.2 us; the launch traced here: 86.1 us
  Pallas kernels  84.5 us (98%)
  local copies, waits for them, and re-layouts  1.57 us (2%)
    pallas_call x1, Pallas kernels, body(): pl.pallas_call(kernel, out_shape=jax.ShapeDtypeStruct((rows, cols), BF16)...  84.5 us

profile of v2, /device:TPU:0, one launch (start us, length us, event | category | flops | bytes accessed | tf_op | source)
XLA Modules:
  0.0 86.1 jit_solution(5173829532896771236)
XLA Ops:
  0.0 84.5 %shard_map.190 = bf16[128,512]{1,0:T(8,128)(2,1)} custom-call(bf16[128,512]{1,0:T(8,128)(2,1)} %refs_0_.1, bf16[128,512]{1,0:T(8,128)(2,1)} %refs_1_.1, bf16[512,128]{1,0:T(8,128)(2,1)} %bitcast.17, bf16[1024,128]{1,0:T(8,128)(2,1)} %bitcast.16, f32[8,128]{1,0:T(8,128)} %bitcast.18, f32[4,128]{1,0:T(4,128)} %bitcast.19, bf16[128,512]{1,0:T(8,128)(2,1)} %refs_6_.1, ...), custom_call_target="tpu_custom_call" | custom-call | tf_op jit(solution)/shard_map/pallas_call | solution.py:1466
  84.5 1.6 %copy.23 = bf16[128,512]{1,0:T(8,128)(2,1)} copy(bf16[128,512]{1,0:T(8,128)(2,1)} %shard_map.190) | data formatting | bytes 262144

commit v3 on v2

--- a/solution.py
+++ b/solution.py
@@ -71,7 +71,7 @@
         ).start()
 
 
-def stats_finish(n_tp, sp, tp, stat, send, recv, rows):
+def stats_rows(n_tp, sp, tp, stat, send, recv):
     for o in range(1, n_tp):
         peer = lax.rem(tp + o, n_tp)
         remote(stat.at[peer], stat.at[peer], send.at[o], recv.at[peer], {"sp": sp, "tp": peer}).wait_recv()
@@ -81,7 +81,12 @@
     total = stat[0]
     for t in range(1, n_tp):
         total = total + stat[t]
-    return column(total[0], rows), column(total[1], rows)
+    return total[0], total[1]
+
+
+def stats_finish(n_tp, sp, tp, stat, send, recv, rows):
+    one, two = stats_rows(n_tp, sp, tp, stat, send, recv)
+    return column(one, rows), column(two, rows)
 
 
 def norm(total, one, two, gain, bias, columns):
@@ -329,7 +334,8 @@
 
 def plane_attend(
     early,
-    between,
+    send_rows,
+    send_scales,
     n_sp,
     n_tp,
     nx,
@@ -371,6 +377,7 @@
     yb,
     part,
     got,
+    across,
     stat1,
     stat2,
     load_sem,
@@ -433,10 +440,10 @@
             remote(*kv, in_send.at[2, dest], in_recv.at[2, sp], where),
         )
 
-    def each_dest(act):
+    def each_dest(act, low, high):
         def hop(t, carry):
             away = (t + 1) // 2
-            zz = z + away * (2 * lax.rem(t, 2) - 1)
+            zz = z + away * (2 * lax.rem(t, 2) - 1) * (1 - 2 * lax.rem(tp, 2))
             for xx in range(nx):
                 there = (zz >= 0) & (zz < nz) & ((zz != z) | (xx != x))
                 for alpha in (True, False):
@@ -448,9 +455,12 @@
 
             return carry
 
-        lax.fori_loop(0, 2 * nz - 1, hop, 0)
-
-    each_dest(lambda copy: copy.start())
+        lax.fori_loop(low, high, hop, 0)
+
+    hops = 2 * nz - 1
+    outer = ((z == 0) | (z == nz - 1)).astype(jnp.int32)
+    held = hops + 0 * outer
+    each_dest(lambda copy: copy.start(), 0, held)
     early()
 
     def o_copy(d):
@@ -545,7 +555,13 @@
             up = jnp.where(lower_half, low == 0, high < nz - 1).astype(jnp.int32)
             first = (k == 0).astype(jnp.int32)
             p = first * z + (1 - first) * (up * (high + 1) + (1 - up) * (low - 1))
+
             arrive(p)
+
+            @pl.when(k == 1)
+            def _():
+                each_dest(lambda copy: copy.start(), held, hops)
+
             step(p, p, True)
             count = (1 - first) * (high - low + 1)
 
@@ -563,8 +579,6 @@
         @pl.when(is_alpha(z, x) == alpha)
         def _(alpha=alpha):
             attend(alpha)
-
-    between()
 
     def o_wait(j, carry):
         @pl.when(j != sp)
@@ -580,39 +594,55 @@
     stats_start(n_tp, sp, tp, lane_sums(aa * aa), lane_sums(ab * ab), stat1, s1_send, s1_recv)
     loads[2].wait()
     loads[3].wait()
+    core = lax.rem(tp, 2)
+    y = tp // 2
+    sides = ((1 - y) * 2, y * 2)
+    to_mate = {"sp": sp, "tp": y * 2 + 1 - core}
+    to_far = {"sp": sp, "tp": (1 - y) * 2 + core}
     na = (aa * ga_ref[...]).astype(BF16)
     nb = (ab * gb_ref[...]).astype(BF16)
-    for t in range(n_tp):
-        ya[t] = jnp.dot(na, pa[:, t * cols : (t + 1) * cols], preferred_element_type=F32)
-        yb[t] = jnp.dot(nb, pb[:, t * cols : (t + 1) * cols], preferred_element_type=F32)
+
+    def project(t):
+        at = pl.ds(pl.multiple_of(t * cols, 128), cols)
+        return (
+            jnp.dot(na, pa[:, at], preferred_element_type=F32),
+            jnp.dot(nb, pb[:, at], preferred_element_type=F32),
+        )
+
+    def mate_copy(k):
+        return remote(part.at[k], got.at[k], part_send.at[k], part_recv.at[k], to_mate)
+
+    for k in range(2):
+        a, b = project(sides[k] + 1 - core)
+        part[k, 0] = a.astype(BF16)
+        part[k, 1] = b.astype(BF16)
+        mate_copy(k).start()
+    for k in range(2):
+        ya[k], yb[k] = project(sides[k] + core)
     sq_a, sq_b = stats_finish(n_tp, sp, tp, stat1, s1_send, s1_recv, rows)
     scale_a = lax.rsqrt(sq_a / (wide * n_tp) + norm_eps)
     scale_b = lax.rsqrt(sq_b / (kvb * 128 * n_tp) + norm_eps)
 
-    def part_copy(o):
-        peer = lax.rem(tp + o, n_tp)
-        return remote(
-            part.at[peer], got.at[tp], part_send.at[o], part_recv.at[tp], {"sp": sp, "tp": peer}
-        )
-
-    for o in range(1, n_tp):
-        peer = lax.rem(tp + o, n_tp)
-        part[peer] = (ya[peer] * scale_a + yb[peer] * scale_b).astype(BF16)
-        part_copy(o).start()
-    total = (ya[tp] * scale_a + yb[tp] * scale_b).astype(BF16).astype(F32)
-    for o in range(1, n_tp):
-        peer = lax.rem(tp + o, n_tp)
-        remote(
-            part.at[peer], got.at[peer], part_send.at[o], part_recv.at[peer], {"sp": sp, "tp": peer}
-        ).wait_recv()
-        total = total + got[peer].astype(F32)
-    mixed = total.astype(BF16).astype(F32)
-    first = depth_scale * res_ref[...].astype(F32) + mixed
-    stats_start(n_tp, sp, tp, lane_sums(first), lane_sums(first * first), stat2, s2_send, s2_recv)
-    for o in range(1, n_tp):
-        part_copy(o).wait_send()
-
-    each_dest(lambda copy: copy.wait_send())
+    def chip_sum(k):
+        mate_copy(k).wait_recv()
+        return (ya[k] + got[k, 0].astype(F32)) * scale_a + (yb[k] + got[k, 1].astype(F32)) * scale_b
+
+    far_copy = remote(across.at[0], across.at[1], part_send.at[2], part_recv.at[2], to_far)
+    across[0] = chip_sum(0).astype(BF16)
+    far_copy.start()
+    total = chip_sum(1)
+    residual = depth_scale * res_ref[...].astype(F32)
+    far_copy.wait_recv()
+    mixed = (total + across[1].astype(F32)).astype(BF16).astype(F32)
+    first = residual + mixed
+    sums = lane_sums(first)
+    stats_start(n_tp, sp, tp, sums, lane_sums(first * first), stat2, s2_send, s2_recv)
+    centre = sums / cols
+    send_rows((first - column(centre, rows)).astype(BF16))
+    far_copy.wait_send()
+    for k in range(2):
+        mate_copy(k).wait_send()
+    each_dest(lambda copy: copy.wait_send(), 0, hops)
 
     def o_drain(j, carry):
         @pl.when(j != sp)
@@ -622,8 +652,13 @@
         return carry
 
     lax.fori_loop(0, n_sp, o_drain, 0)
-    one, two = stats_finish(n_tp, sp, tp, stat2, s2_send, s2_recv, rows)
-    out_ref[...] = norm(first, one, two, gs_ref[...], bs_ref[...], cols * n_tp)
+    one, two = stats_rows(n_tp, sp, tp, stat2, s2_send, s2_recv)
+    mean = one / (cols * n_tp)
+    factor = lax.rsqrt(two / (cols * n_tp) - mean * mean + norm_eps)
+    shifts = [(stat2[t, 0] / cols - mean) * factor for t in range(n_tp)]
+    send_scales([factor] + shifts)
+    flat = (first - column(mean, rows)) * column(factor, rows)
+    out_ref[...] = (flat * gs_ref[...] + bs_ref[...]).astype(BF16)
 
 
 def expert_kernel(
@@ -907,6 +942,8 @@
     nx,
     cap,
     set_ref,
+    gs_ref,
+    bs_ref,
     ids_ref,
     weight_ref,
     wg_hbm,
@@ -919,10 +956,10 @@
     wu,
     wd,
     hits,
-    wpack,
-    wrecv,
-    wcol,
     packed,
+    scales,
+    scaled,
+    affine,
     xbuf,
     gate,
     up,
@@ -940,10 +977,12 @@
     back,
     stat,
     load_sem,
-    w_send,
-    w_recv,
     a_send,
     a_recv,
+    t_send,
+    t_recv,
+    g_send,
+    g_recv,
     x_send,
     x_recv,
     d_send,
@@ -983,8 +1022,9 @@
         pltpu.make_async_copy(wd_hbm.at[0], wd, load_sem.at[2]),
     )
 
-    def w_copy(d):
-        return remote(wpack.at[d // nx], wrecv.at[sp], w_send.at[d], w_recv.at[sp], {"sp": d, "tp": tp})
+    def g_copy(o):
+        where = {"sp": sp, "tp": lax.rem(tp + o, n_tp)}
+        return remote(affine.at[tp], affine.at[tp], g_send.at[o], g_recv.at[tp], where)
 
     def others(fn):
         def one(d, carry):
@@ -999,6 +1039,10 @@
     def early():
         for load in loads:
             load.start()
+        affine[tp, 0:1] = gs_ref[...]
+        affine[tp, 1:2] = bs_ref[...]
+        for o in range(1, n_tp):
+            g_copy(o).start()
         ids = [ids_ref[k : k + 1, :] for k in range(2)]
         r = lax.broadcasted_iota(jnp.int32, (rows, rows), 0)
         c = lax.broadcasted_iota(jnp.int32, (rows, rows), 1)
@@ -1010,46 +1054,45 @@
         for g in range(nz):
             match = jnp.where(seat == before[g : g + 1], hot[g : g + 1], 0.0).astype(BF16)
             hits[g * cap : (g + 1) * cap] = match
-            share = [
-                jnp.where(ids[0] == g * nx + e, weight_ref[0:1, :], 0.0)
-                + jnp.where(ids[1] == g * nx + e, weight_ref[1:2, :], 0.0)
-                for e in range(nx)
-            ]
-            line = lax.broadcasted_iota(jnp.int32, (8, rows), 0)
-            both = jnp.where(line == 0, share[0], jnp.where(line == 1, share[1], 0.0))
-            high, low = split(both)
-            dims = (((1,), (1,)), ((), ()))
-            wpack[g] = jnp.zeros((8, 128), F32)
-            wpack[g, :, 0:cap] = lax.dot_general(high, match, dims, preferred_element_type=F32) + lax.dot_general(
-                low, match, dims, preferred_element_type=F32
-            )
-        others(lambda d: w_copy(d).start())
-        wrecv[sp] = wpack[z]
-
-    def between():
-        def spread(j, carry):
-            @pl.when(j != sp)
-            def _():
-                remote(wrecv.at[j], wrecv.at[j], w_send.at[0], w_recv.at[j], {"sp": sp, "tp": tp}).wait_recv()
-
-            wide = jnp.transpose(jnp.broadcast_to(wrecv[j, pl.ds(x, 1), :], (128, 128)))
-            wcol[lax.rem(j, nx), j // nx] = wide[0:cap]
-            return carry
-
-        lax.fori_loop(0, n_sp, spread, 0)
-
-    attention(early, between)
-
-    sent = jnp.dot(hits[...], set_ref[...], preferred_element_type=F32).astype(BF16)
-    packed[...] = sent.reshape(nz, cap, cols)
+            scales[g] = jnp.zeros((8, 128), F32)
 
     def a_copy(i):
         g = near(i)
         return remote(packed.at[g], xbuf.at[tp, x, z], a_send.at[i], a_recv.at[z], {"sp": g * nx + x, "tp": tp})
 
-    for i in range(1, nz):
-        a_copy(i).start()
-    xbuf[tp, x, z] = packed[z]
+    def t_copy(d):
+        return remote(scales.at[d // nx], scaled.at[sp], t_send.at[d], t_recv.at[sp], {"sp": d, "tp": tp})
+
+    def send_rows(part):
+        sent = jnp.dot(hits[...], part, preferred_element_type=F32).astype(BF16)
+        packed[...] = sent.reshape(nz, cap, cols)
+        for i in range(1, nz):
+            a_copy(i).start()
+        xbuf[tp, x, z] = packed[z]
+
+    def compact(lines, g):
+        line = lax.broadcasted_iota(jnp.int32, (8, rows), 0)
+        tile = jnp.zeros((8, rows), F32)
+        for k, value in enumerate(lines):
+            tile = jnp.where(line == k, value, tile)
+        high, low = split(tile)
+        dims = (((1,), (1,)), ((), ()))
+        match = hits[g * cap : (g + 1) * cap]
+        return lax.dot_general(high, match, dims, preferred_element_type=F32) + lax.dot_general(
+            low, match, dims, preferred_element_type=F32
+        )
+
+    def send_scales(lines):
+        for g in range(nz):
+            share = []
+            for e in range(nx):
+                chosen = [
+                    jnp.where(ids_ref[k : k + 1, :] == g * nx + e, weight_ref[k : k + 1, :], 0.0) for k in range(2)
+                ]
+                share.append(chosen[0] + chosen[1])
+            scales[g, :, 0:cap] = compact(lines + share, g)
+        others(lambda d: t_copy(d).start())
+        scaled[sp] = scales[z]
 
     def x_copy(kind, t, xs, g, where):
         block = xbuf.at[t, xs, g]
@@ -1087,8 +1130,27 @@
         x_wait(far, 1 - x, g)
         x_copy(7, far, 1 - x, g, to_mate).start()
 
+    def t_wait(j):
+        remote(scaled.at[j], scaled.at[j], t_send.at[0], t_recv.at[j], to_mate).wait_recv()
+
     def piece(t, xs, fresh):
-        block = xbuf[t, xs].reshape(nz * cap, cols)
+        factor, shift = [], []
+        for g in range(nz):
+            j = g * nx + xs
+            factor.append(scaled[j, 0:1, :])
+            shift.append(scaled[j, pl.ds(1 + t, 1), :])
+        turned = jnp.transpose(jnp.concatenate(factor + shift, axis=0))
+        gain, bias = affine[t, 0:1, :], affine[t, 1:2, :]
+        block = jnp.concatenate(
+            [
+                (
+                    (xbuf[t, xs, g].astype(F32) * turned[0:cap, g : g + 1] + turned[0:cap, nz + g : nz + g + 1]) * gain
+                    + bias
+                ).astype(BF16)
+                for g in range(nz)
+            ],
+            axis=0,
+        )
         at = pl.ds(pl.multiple_of(t * cols, 128), cols)
         g = jnp.dot(block, wg[at, :], preferred_element_type=F32)
         u = jnp.dot(block, wu[at, :], preferred_element_type=F32)
@@ -1106,22 +1168,35 @@
 
         lax.fori_loop(0, nz, one, 0)
 
-    for i in range(nz + 2):
+    def exchange(i):
         if i < nz:
             own_out(i)
         if 1 <= i <= nz:
             pass_on(i - 1)
         if i >= 2:
             pass_diag(i - 2)
+
+    def first_rows(part):
+        send_rows(part)
+        exchange(0)
+        exchange(1)
+
+    attention(early, first_rows, send_scales)
+    for i in range(2, nz + 2):
+        exchange(i)
         if i == nz - 1:
             loads[0].wait()
             loads[1].wait()
+            others(t_wait)
+            for o in range(1, n_tp):
+                peer = lax.rem(tp + o, n_tp)
+                remote(affine.at[peer], affine.at[peer], g_send.at[0], g_recv.at[peer], to_mate).wait_recv()
             piece(tp, x, True)
         if i == nz:
             all_in(mate, x)
             piece(mate, x, False)
+            piece(far, x, False)
             piece(tp, 1 - x, True)
-    piece(far, x, False)
     all_in(far_mate, x)
     piece(far_mate, x, False)
     all_in(mate, 1 - x)
@@ -1131,7 +1206,9 @@
     piece(far_mate, 1 - x, False)
     for xs in range(nx):
         value = gate[xs]
-        weight = jnp.concatenate([wcol[xs].reshape(nz * cap, 128)] * (value.shape[1] // 128), axis=1)
+        line = [scaled[g * nx + xs, pl.ds(1 + n_tp + x, 1), :] for g in range(nz)]
+        turned = jnp.transpose(jnp.concatenate(line + line, axis=0))
+        weight = jnp.concatenate([turned[0:cap, g : g + 1] for g in range(nz)], axis=0)
         hid[xs * nz * cap : (xs + 1) * nz * cap] = (value / (1.0 + jnp.exp(-value)) * up[xs] * weight).astype(BF16)
     loads[2].wait()
 
@@ -1167,42 +1244,57 @@
         return m_copy(2, midy, goty, g, to_y)
 
     order = range(nz - 1, -1, -1)
+    late = order[nz // 2 :]
+
+    def plain(i):
+        g = near(i)
+
+        def plain_x():
+            midx[g] = pair(0, 1 - x, g).astype(BF16)
+            x_send_copy(g).start()
+
+        def plain_y():
+            midy[g] = pair(1, x, g).astype(BF16)
+            y_send_copy(g).start()
+
+        when_x_first(g, plain_x)
+        when_y_first(g, plain_y)
+
+    def joined(i):
+        g = near(i)
+        diag_copy(g, to_mate).wait_recv()
+
+        def joined_y():
+            midy[g] = (pair(1, x, g) + gotd[g].astype(F32)).astype(BF16)
+            y_send_copy(g).start()
+
+        def joined_x():
+            midx[g] = (pair(0, 1 - x, g) + gotd[g].astype(F32)).astype(BF16)
+            x_send_copy(g).start()
+
+        when_x_first(g, joined_y)
+        when_y_first(g, joined_x)
+
+    def diagonal(i):
+        g = near(i)
+        mid[g] = pair(1, 1 - x, g).astype(BF16)
+        when_x_first(g, lambda: diag_copy(g, to_x).start())
+        when_y_first(g, lambda: diag_copy(g, to_y).start())
+
     d_copy(1, 1 - x).wait_recv()
     for i in order:
-        g = near(i)
-        mid[g] = pair(1, 1 - x, g).astype(BF16)
-        when_x_first(g, lambda g=g: diag_copy(g, to_x).start())
-        when_y_first(g, lambda g=g: diag_copy(g, to_y).start())
+        diagonal(i)
     home[0] = down(tp)
     d_copy(1, x).wait_recv()
     d_copy(0, 1 - x).wait_recv()
-    for i in order:
-        g = near(i)
-
-        def plain_x(g=g):
-            midx[g] = pair(0, 1 - x, g).astype(BF16)
-            x_send_copy(g).start()
-
-        def plain_y(g=g):
-            midy[g] = pair(1, x, g).astype(BF16)
-            y_send_copy(g).start()
-
-        when_x_first(g, plain_x)
-        when_y_first(g, plain_y)
-    for i in order:
-        g = near(i)
-        diag_copy(g, to_mate).wait_recv()
-
-        def joined_y(g=g):
-            midy[g] = (pair(1, x, g) + gotd[g].astype(F32)).astype(BF16)
-            y_send_copy(g).start()
-
-        def joined_x(g=g):
-            midx[g] = (pair(0, 1 - x, g) + gotd[g].astype(F32)).astype(BF16)
-            x_send_copy(g).start()
-
-        when_x_first(g, joined_y)
-        when_y_first(g, joined_x)
+    for i in order[: nz // 2]:
+        plain(i)
+    for i in order[: nz // 2]:
+        joined(i)
+    for i in late:
+        plain(i)
+    for i in late:
+        joined(i)
 
     def b_copy(i):
         g = near(i)
@@ -1226,7 +1318,9 @@
     routed = lax.dot_general(hits[...], flat, (((0,), (0,)), ((), ())), preferred_element_type=F32)
     second = depth_scale * set_ref[...].astype(F32) + routed
     stats_start(n_tp, sp, tp, lane_sums(second), lane_sums(second * second), stat, s_send, s_recv)
-    others(lambda d: w_copy(d).wait_send())
+    others(lambda d: t_copy(d).wait_send())
+    for o in range(1, n_tp):
+        g_copy(o).wait_send()
     for i in range(nz):
         g = near(i)
         if i:
@@ -1315,7 +1409,7 @@
         DMA((n_tp,)),
         DMA((n_tp,)),
     ]
-    balanced = nx == 2 and ny == 2 and kva == nz and kvb == nz and cap % 16 == 0
+    balanced = (nx, ny, kva, kvb) == (2, 2, nz, nz)
     tall = nx * rows
     plane_scratch = [
         VMEM((rows * kva, 128), BF16),
@@ -1336,10 +1430,11 @@
         VMEM((n_sp, rows, 128), BF16),
         VMEM(project_alpha.shape, BF16),
         VMEM(project_beta.shape, BF16),
-        VMEM((n_tp, rows, cols), F32),
-        VMEM((n_tp, rows, cols), F32),
-        VMEM((n_tp, rows, cols), BF16),
-        VMEM((n_tp, rows, cols), BF16),
+        VMEM((ny, rows, cols), F32),
+        VMEM((ny, rows, cols), F32),
+        VMEM((ny, 2, rows, cols), BF16),
+        VMEM((ny, 2, rows, cols), BF16),
+        VMEM((2, rows, cols), BF16),
         VMEM((n_tp, 2, 8, rows), F32),
         VMEM((n_tp, 2, 8, rows), F32),
         DMA((4,)),
@@ -1392,10 +1487,10 @@
         VMEM((width, units), BF16),
         VMEM((units, width), BF16),
         VMEM((nz * cap, rows), BF16),
+        VMEM(block, BF16),
         VMEM((nz, 8, 128), F32),
         VMEM((n_sp, 8, 128), F32),
-        VMEM((nx, nz, cap, 128), F32),
-        VMEM(block, BF16),
+        VMEM((n_tp, 8, cols), F32),
         VMEM((n_tp, nx) + block, BF16),
         VMEM((nx, nz * cap, units), F32),
         VMEM((nx, nz * cap, units), F32),
@@ -1413,10 +1508,12 @@
         VMEM(block, BF16),
         VMEM((n_tp, 2, 8, rows), F32),
         DMA((3,)),
+        DMA((nz,)),
+        DMA((nz,)),
         DMA((n_sp,)),
         DMA((n_sp,)),
-        DMA((nz,)),
-        DMA((nz,)),
+        DMA((n_tp,)),
+        DMA((n_tp,)),
         DMA((8, nz)),
         DMA((n_tp, nx, nz)),
         DMA((ny, nx)),
@@ -1460,6 +1557,8 @@
             attend = plane_attend if balanced else attend_kernel
             attend(*hooks, n_sp, n_tp, nx, kva, kvb, *attend_in, settled, *own[:n_attend])
 
+        if balanced:
+            expert_in = attend_in[-2:] + expert_in
         expert = plane_expert if balanced else expert_kernel
         expert(attention, n_sp, n_tp, nx, cap, settled, *expert_in, out_ref, *own[n_attend:])
 

time: 86.2 us -> 81 us (0.940)
  Pallas kernels: 84.5 us -> 79.2 us
    pallas_call x1, Pallas kernels: 84.5 us -> 79.2 us  [body(): pl.pallas_call(kernel, out_shape=jax.ShapeDtypeStruct((rows, cols), BF16)...]
where the time goes in v3:
time: 81 us; the launch traced here: 80.8 us
  Pallas kernels  79.2 us (98%)
  local copies, waits for them, and re-layouts  1.57 us (2%)
    pallas_call x1, Pallas kernels, body(): pl.pallas_call(kernel, out_shape=jax.ShapeDtypeStruct((rows, cols), BF16)...  79.2 us

profile of v3, /device:TPU:0, one launch (start us, length us, event | category | flops | bytes accessed | tf_op | source)
XLA Modules:
  0.0 80.8 jit_solution(13846153254127868261)
XLA Ops:
  0.0 79.2 %shard_map.190 = bf16[128,512]{1,0:T(8,128)(2,1)} custom-call(bf16[128,512]{1,0:T(8,128)(2,1)} %refs_0_.1, bf16[128,512]{1,0:T(8,128)(2,1)} %refs_1_.1, bf16[512,128]{1,0:T(8,128)(2,1)} %bitcast.17, bf16[1024,128]{1,0:T(8,128)(2,1)} %bitcast.16, f32[8,128]{1,0:T(8,128)} %bitcast.18, f32[4,128]{1,0:T(4,128)} %bitcast.19, bf16[128,512]{1,0:T(8,128)(2,1)} %refs_6_.1, ...), custom_call_target="tpu_custom_call" | custom-call | tf_op jit(solution)/shard_map/pallas_call | solution.py:1565
  79.2 1.6 %copy.23 = bf16[128,512]{1,0:T(8,128)(2,1)} copy(bf16[128,512]{1,0:T(8,128)(2,1)} %shard_map.190) | data formatting | bytes 262144

commit v4 on v3

--- a/solution.py
+++ b/solution.py
@@ -62,9 +62,9 @@
     return jnp.transpose(jnp.broadcast_to(row[0:1, :], (rows, rows)))[:, 0:1]
 
 
-def stats_start(n_tp, sp, tp, one, two, stat, send, recv):
-    stat[tp, 0] = one
-    stat[tp, 1] = two
+def stats_start(n_tp, sp, tp, one, two, stat, send, recv, *more):
+    for k, value in enumerate((one, two) + more):
+        stat[tp, k] = value
     for o in range(1, n_tp):
         remote(
             stat.at[tp], stat.at[tp], send.at[o], recv.at[tp], {"sp": sp, "tp": lax.rem(tp + o, n_tp)}
@@ -336,6 +336,7 @@
     early,
     send_rows,
     send_scales,
+    small_loads,
     n_sp,
     n_tp,
     nx,
@@ -412,10 +413,14 @@
     )
     loads[0].start()
     loads[1].start()
+    for load in small_loads:
+        load.start()
+    greet(n_sp, n_tp, sp, tp)
+    for load in small_loads:
+        load.wait()
     for u in range(nz):
-        own_off[u, 0:2] = offa_ref[2 * u : 2 * u + 2]
-        own_off[u, 2:3] = offb_ref[u : u + 1]
-    greet(n_sp, n_tp, sp, tp)
+        own_off[0, u] = offa_ref[2 * u : 2 * u + 2]
+        own_off[1, u] = jnp.broadcast_to(offb_ref[u : u + 1], (2, 128))
     loads[0].wait()
     wide_a[...] = raw_a[...].astype(F32)
     for u in range(kva):
@@ -435,7 +440,7 @@
         q_ref = qa_ref if alpha else qb_ref
         kv = (own_a.at[zz], kin.at[0, sp]) if alpha else (own_b.at[zz], kin.at[:, sp])
         return (
-            remote(own_off.at[zz], oin.at[sp], in_send.at[0, dest], in_recv.at[0, sp], where),
+            remote(own_off.at[0 if alpha else 1, zz], oin.at[sp], in_send.at[0, dest], in_recv.at[0, sp], where),
             remote(q_ref.at[:, at], qin.at[sp], in_send.at[1, dest], in_recv.at[1, sp], where),
             remote(*kv, in_send.at[2, dest], in_recv.at[2, sp], where),
         )
@@ -458,9 +463,7 @@
         lax.fori_loop(low, high, hop, 0)
 
     hops = 2 * nz - 1
-    outer = ((z == 0) | (z == nz - 1)).astype(jnp.int32)
-    held = hops + 0 * outer
-    each_dest(lambda copy: copy.start(), 0, held)
+    each_dest(lambda copy: copy.start(), 0, hops)
     early()
 
     def o_copy(d):
@@ -475,7 +478,7 @@
         heads = 2 if alpha else 1
         scale = 64**-0.5 if alpha else 128**-0.5
         at = pl.ds(pl.multiple_of(z * 128, 128), 128)
-        oin[sp] = own_off[z]
+        oin[sp] = own_off[0 if alpha else 1, z]
         if alpha:
             qin[sp] = qa_ref[:, at]
             kin[0, sp] = own_a[z]
@@ -514,7 +517,7 @@
             valid = lane_t < row_t
             ws = []
             for h in range(heads):
-                row = h if alpha else 2
+                row = h
                 offset = jnp.concatenate([oin[c * nx + i, row : row + 1, :] for i in range(nx)], axis=1)
                 s = scores[:, h * tall : (h + 1) * tall] * scale + offset
                 soft = jnp.maximum(s, 0.0) + jnp.log(1.0 + jnp.exp(-jnp.abs(s)))
@@ -535,9 +538,10 @@
             o = o if diag else acc[r] + o
             acc[r] = o
 
+        def finish(r, c):
             @pl.when(c == 0)
             def _():
-                obuf[pl.ds(r * nx, nx)] = o.astype(BF16).reshape(nx, rows, 128)
+                obuf[pl.ds(r * nx, nx)] = acc[r].astype(BF16).reshape(nx, rows, 128)
                 for xx in range(nx):
                     d = r * nx + xx
 
@@ -558,18 +562,36 @@
 
             arrive(p)
 
-            @pl.when(k == 1)
+
+            def at(t):
+                return p + t * (1 - up), p - t * up
+
+            @pl.when(k == 0)
             def _():
-                each_dest(lambda copy: copy.start(), held, hops)
-
-            step(p, p, True)
-            count = (1 - first) * (high - low + 1)
-
-            def more(t, carry):
-                step(p + t * (1 - up), p - t * up, False)
+                step(p, p, True)
+                finish(p, p)
+
+            @pl.when(k > 0)
+            def _():
+                step(p, p, True)
+                step(*at(1), False)
+                finish(p, p)
+                finish(*at(1))
+
+            def two(i, carry):
+                step(*at(2 * i), False)
+                step(*at(2 * i + 1), False)
+                finish(*at(2 * i))
+                finish(*at(2 * i + 1))
                 return carry
 
-            lax.fori_loop(1, count + 1, more, 0)
+            lax.fori_loop(1, (k + 1) // 2, two, 0)
+
+            @pl.when((k > 0) & (lax.rem(k, 2) == 0))
+            def _():
+                step(*at(k), False)
+                finish(*at(k))
+
             return jnp.minimum(low, p), jnp.maximum(high, p)
 
         lax.fori_loop(0, nz, phase, (z, z))
@@ -627,20 +649,36 @@
         mate_copy(k).wait_recv()
         return (ya[k] + got[k, 0].astype(F32)) * scale_a + (yb[k] + got[k, 1].astype(F32)) * scale_b
 
-    far_copy = remote(across.at[0], across.at[1], part_send.at[2], part_recv.at[2], to_far)
+    half = cols // 2
     across[0] = chip_sum(0).astype(BF16)
-    far_copy.start()
+
+    def far_copy(k):
+        at = slice(k * half, (k + 1) * half)
+        return remote(
+            across.at[0, :, at], across.at[1, :, at], part_send.at[2 + k], part_recv.at[2 + k], to_far
+        )
+
+    far_copy(0).start()
+    far_copy(1).start()
     total = chip_sum(1)
     residual = depth_scale * res_ref[...].astype(F32)
-    far_copy.wait_recv()
-    mixed = (total + across[1].astype(F32)).astype(BF16).astype(F32)
-    first = residual + mixed
-    sums = lane_sums(first)
-    stats_start(n_tp, sp, tp, sums, lane_sums(first * first), stat2, s2_send, s2_recv)
-    centre = sums / cols
-    send_rows((first - column(centre, rows)).astype(BF16))
-    far_copy.wait_send()
+    firsts, sums, squares = [], [], []
     for k in range(2):
+        at = slice(k * half, (k + 1) * half)
+        far_copy(k).wait_recv()
+        mixed = (total[:, at] + across[1, :, at].astype(F32)).astype(BF16).astype(F32)
+        firsts.append(residual[:, at] + mixed)
+        sums.append(lane_sums(firsts[k]))
+        squares.append(lane_sums(firsts[k] * firsts[k]))
+        if k == 0:
+            centre = sums[0] / half
+            middle = column(centre, rows)
+        else:
+            stats_start(n_tp, sp, tp, sums[0] + sums[1], squares[0] + squares[1], stat2, s2_send, s2_recv, centre)
+        send_rows((firsts[k] - middle).astype(BF16), k)
+    first = jnp.concatenate(firsts, axis=1)
+    for k in range(2):
+        far_copy(k).wait_send()
         mate_copy(k).wait_send()
     each_dest(lambda copy: copy.wait_send(), 0, hops)
 
@@ -655,7 +693,8 @@
     one, two = stats_rows(n_tp, sp, tp, stat2, s2_send, s2_recv)
     mean = one / (cols * n_tp)
     factor = lax.rsqrt(two / (cols * n_tp) - mean * mean + norm_eps)
-    shifts = [(stat2[t, 0] / cols - mean) * factor for t in range(n_tp)]
+    centres = [stat2[t, 2] for t in range(n_tp)]
+    shifts = [(centres[t] - mean) * factor for t in range(n_tp)]
     send_scales([factor] + shifts)
     flat = (first - column(mean, rows)) * column(factor, rows)
     out_ref[...] = (flat * gs_ref[...] + bs_ref[...]).astype(BF16)
@@ -1056,19 +1095,29 @@
             hits[g * cap : (g + 1) * cap] = match
             scales[g] = jnp.zeros((8, 128), F32)
 
-    def a_copy(i):
+    def a_copy(i, k):
         g = near(i)
-        return remote(packed.at[g], xbuf.at[tp, x, z], a_send.at[i], a_recv.at[z], {"sp": g * nx + x, "tp": tp})
+        at = slice(k * half, (k + 1) * half)
+        return remote(
+            packed.at[g, :, at],
+            xbuf.at[tp, x, z, :, at],
+            a_send.at[k, i],
+            a_recv.at[k, z],
+            {"sp": g * nx + x, "tp": tp},
+        )
 
     def t_copy(d):
         return remote(scales.at[d // nx], scaled.at[sp], t_send.at[d], t_recv.at[sp], {"sp": d, "tp": tp})
 
-    def send_rows(part):
+    half = cols // 2
+
+    def send_rows(part, k):
         sent = jnp.dot(hits[...], part, preferred_element_type=F32).astype(BF16)
-        packed[...] = sent.reshape(nz, cap, cols)
+        at = slice(k * half, (k + 1) * half)
+        packed[:, :, at] = sent.reshape(nz, cap, half)
         for i in range(1, nz):
-            a_copy(i).start()
-        xbuf[tp, x, z] = packed[z]
+            a_copy(i, k).start()
+        xbuf[tp, x, z, :, at] = packed[z, :, at]
 
     def compact(lines, g):
         line = lax.broadcasted_iota(jnp.int32, (8, rows), 0)
@@ -1111,7 +1160,9 @@
     def own_out(i):
         g = near(i)
         if i:
-            remote(packed.at[g], xbuf.at[tp, x, g], a_send.at[0], a_recv.at[g], to_mate).wait_recv()
+            for k in range(2):
+                block = xbuf.at[tp, x, g, :, k * half : (k + 1) * half]
+                remote(block, block, a_send.at[0, 0], a_recv.at[k, g], to_mate).wait_recv()
         x_copy(1, tp, x, g, to_x).start()
         x_copy(2, tp, x, g, to_y).start()
         x_copy(0, tp, x, g, to_mate).start()
@@ -1168,35 +1219,35 @@
 
         lax.fori_loop(0, nz, one, 0)
 
-    def exchange(i):
-        if i < nz:
-            own_out(i)
-        if 1 <= i <= nz:
+    def first_rows(part, k):
+        send_rows(part, k)
+        if k == 1:
+            own_out(0)
+            own_out(1)
+            pass_on(0)
+
+    attention(early, first_rows, send_scales)
+    for i in range(2, nz):
+        own_out(i)
+        if i < nz - 1:
             pass_on(i - 1)
-        if i >= 2:
             pass_diag(i - 2)
-
-    def first_rows(part):
-        send_rows(part)
-        exchange(0)
-        exchange(1)
-
-    attention(early, first_rows, send_scales)
-    for i in range(2, nz + 2):
-        exchange(i)
-        if i == nz - 1:
-            loads[0].wait()
-            loads[1].wait()
-            others(t_wait)
-            for o in range(1, n_tp):
-                peer = lax.rem(tp + o, n_tp)
-                remote(affine.at[peer], affine.at[peer], g_send.at[0], g_recv.at[peer], to_mate).wait_recv()
-            piece(tp, x, True)
-        if i == nz:
-            all_in(mate, x)
-            piece(mate, x, False)
-            piece(far, x, False)
-            piece(tp, 1 - x, True)
+    loads[0].wait()
+    loads[1].wait()
+    others(t_wait)
+    for o in range(1, n_tp):
+        peer = lax.rem(tp + o, n_tp)
+        remote(affine.at[peer], affine.at[peer], g_send.at[0], g_recv.at[peer], to_mate).wait_recv()
+    piece(tp, x, True)
+    pass_on(nz - 2)
+    pass_diag(nz - 3)
+    all_in(mate, x)
+    piece(mate, x, False)
+    pass_on(nz - 1)
+    pass_diag(nz - 2)
+    piece(tp, 1 - x, True)
+    piece(far, x, False)
+    pass_diag(nz - 1)
     all_in(far_mate, x)
     piece(far_mate, x, False)
     all_in(mate, 1 - x)
@@ -1324,7 +1375,8 @@
     for i in range(nz):
         g = near(i)
         if i:
-            a_copy(i).wait_send()
+            a_copy(i, 0).wait_send()
+            a_copy(i, 1).wait_send()
             b_copy(i).wait_send()
         x_copy(1, tp, x, g, to_x).wait_send()
         x_copy(2, tp, x, g, to_y).wait_send()
@@ -1418,10 +1470,10 @@
         VMEM((rows * kvb * 2, 128), F32),
         VMEM((kva, rows, 128), BF16),
         VMEM((kvb, 2, rows, 128), BF16),
-        VMEM((nz, 8, 128), F32),
+        VMEM((2, nz, 2, 128), F32),
         VMEM((n_sp, rows, 128), BF16),
         VMEM((2, n_sp, rows, 128), BF16),
-        VMEM((n_sp, 8, 128), F32),
+        VMEM((n_sp, 2, 128), F32),
         VMEM((nz, 2 * tall, 128), BF16),
         VMEM((nz, 2 * tall, 128), BF16),
         VMEM((2, nz, tall, 128), F32),
@@ -1436,7 +1488,7 @@
         VMEM((ny, 2, rows, cols), BF16),
         VMEM((2, rows, cols), BF16),
         VMEM((n_tp, 2, 8, rows), F32),
-        VMEM((n_tp, 2, 8, rows), F32),
+        VMEM((n_tp, 3, 8, rows), F32),
         DMA((4,)),
         DMA((3, n_sp)),
         DMA((3, n_sp)),
@@ -1508,8 +1560,8 @@
         VMEM(block, BF16),
         VMEM((n_tp, 2, 8, rows), F32),
         DMA((3,)),
-        DMA((nz,)),
-        DMA((nz,)),
+        DMA((2, nz)),
+        DMA((2, nz)),
         DMA((n_sp,)),
         DMA((n_sp,)),
         DMA((n_tp,)),
@@ -1548,30 +1600,26 @@
     n_all = n_in + len(routes) + 5
 
     def kernel(*refs):
+        refs = list(refs)
+        loads = []
+        for k, i in enumerate(small):
+            loads.append(pltpu.make_async_copy(refs[i], refs[k - len(small) - 1], refs[-1].at[k]))
+            refs[i] = refs[k - len(small) - 1]
         attend_in = refs[:n_in]
         out_ref, settled = refs[n_all : n_all + 2]
         expert_in = refs[n_in:n_all]
-        own = refs[n_all + 2 :]
+        own = refs[n_all + 2 : len(refs) - (len(small) + 1 if small else 0)]
 
         def attention(*hooks):
             attend = plane_attend if balanced else attend_kernel
-            attend(*hooks, n_sp, n_tp, nx, kva, kvb, *attend_in, settled, *own[:n_attend])
+            attend(*hooks, *(loads,) * balanced, n_sp, n_tp, nx, kva, kvb, *attend_in, settled, *own[:n_attend])
 
         if balanced:
             expert_in = attend_in[-2:] + expert_in
         expert = plane_expert if balanced else expert_kernel
         expert(attention, n_sp, n_tp, nx, cap, settled, *expert_in, out_ref, *own[n_attend:])
 
-    return pl.pallas_call(
-        kernel,
-        out_shape=jax.ShapeDtypeStruct((rows, cols), BF16),
-        in_specs=[vm, vm, hbm, hbm] + places_in + [vm] * 3 + [hbm] * 2 + [vm] * (2 + len(routes)) + [hbm] * 3 + [vm] * 2,
-        out_specs=vm,
-        scratch_shapes=[VMEM((rows, cols), BF16)] + attend_scratch + expert_scratch,
-        compiler_params=pltpu.CompilerParams(
-            collective_id=0, has_side_effects=True, vmem_limit_bytes=60 * 1024 * 1024
-        ),
-    )(
+    operands = [
         query_alpha,
         query_beta,
         *keyed,
@@ -1588,7 +1636,23 @@
         expert_down,
         row(gain_final),
         row(bias_final),
-    )
+    ]
+    specs = [vm, vm, hbm, hbm] + places_in + [vm] * 3 + [hbm] * 2 + [vm] * (2 + len(routes)) + [hbm] * 3 + [vm] * 2
+    small = [i for i, spec in enumerate(specs) if spec is vm] if balanced else []
+    scratch = [VMEM((rows, cols), BF16)] + attend_scratch + expert_scratch
+    if small:
+        scratch = scratch + [VMEM(operands[i].shape, operands[i].dtype) for i in small] + [DMA((len(small),))]
+        specs = [hbm] * len(specs)
+    return pl.pallas_call(
+        kernel,
+        out_shape=jax.ShapeDtypeStruct((rows, cols), BF16),
+        in_specs=specs,
+        out_specs=vm,
+        scratch_shapes=scratch,
+        compiler_params=pltpu.CompilerParams(
+            collective_id=0, has_side_effects=True, vmem_limit_bytes=60 * 1024 * 1024
+        ),
+    )(*operands)
 
 
 def solution(mesh):

time: 81 us -> 79.1 us (0.977)
  Pallas kernels: 79.2 us -> 77.4 us
    pallas_call x1, Pallas kernels: 79.2 us -> 77.4 us  [body(): pl.pallas_call(kernel, out_shape=jax.ShapeDtypeStruct((rows, cols), BF16)...]
where the time goes in v4:
time: 79.1 us; the launch traced here: 79 us
  Pallas kernels  77.4 us (98%)
  local copies, waits for them, and re-layouts  1.57 us (2%)
    pallas_call x1, Pallas kernels, body(): pl.pallas_call(kernel, out_shape=jax.ShapeDtypeStruct((rows, cols), BF16)...  77.4 us

profile of v4, /device:TPU:0, one launch (start us, length us, event | category | flops | bytes accessed | tf_op | source)
XLA Modules:
  0.0 79.0 jit_solution(8852990703886574473)
XLA Ops:
  0.0 77.4 %shard_map.190 = bf16[128,512]{1,0:T(8,128)(2,1)} custom-call(bf16[128,512]{1,0:T(8,128)(2,1)} %refs_0_.1, bf16[128,512]{1,0:T(8,128)(2,1)} %refs_1_.1, bf16[512,128]{1,0:T(8,128)(2,1)} %bitcast.17, bf16[1024,128]{1,0:T(8,128)(2,1)} %bitcast.16, f32[8,128]{1,0:T(8,128)} %bitcast.18, f32[4,128]{1,0:T(4,128)} %bitcast.19, bf16[128,512]{1,0:T(8,128)(2,1)} %refs_6_.1, ...), custom_call_target="tpu_custom_call" | custom-call | tf_op jit(solution)/shard_map/pallas_call | solution.py:1646
  77.4 1.6 %copy.23 = bf16[128,512]{1,0:T(8,128)(2,1)} copy(bf16[128,512]{1,0:T(8,128)(2,1)} %shard_map.190) | data formatting | bytes 262144

commit v5 on v4

--- a/solution.py
+++ b/solution.py
@@ -447,10 +447,13 @@
 
     def each_dest(act, low, high):
         def hop(t, carry):
-            away = (t + 1) // 2
-            zz = z + away * (2 * lax.rem(t, 2) - 1) * (1 - 2 * lax.rem(tp, 2))
-            for xx in range(nx):
-                there = (zz >= 0) & (zz < nz) & ((zz != z) | (xx != x))
+            zz = z
+            for a in range(nz):
+                for i, g in enumerate(sorted(range(nz), key=lambda g: (min(g, nz - 1 - g), abs(g - a)))):
+                    zz = jnp.where((z == a) & (t == i), g, zz)
+            for step in range(nx):
+                xx = lax.rem(x + step + lax.rem(tp, 2), nx)
+                there = (zz != z) | (xx != x)
                 for alpha in (True, False):
 
                     @pl.when(there & (is_alpha(zz, xx) == alpha))
@@ -462,7 +465,7 @@
 
         lax.fori_loop(low, high, hop, 0)
 
-    hops = 2 * nz - 1
+    hops = nz
     each_dest(lambda copy: copy.start(), 0, hops)
     early()
 
@@ -1247,9 +1250,9 @@
     pass_diag(nz - 2)
     piece(tp, 1 - x, True)
     piece(far, x, False)
-    pass_diag(nz - 1)
     all_in(far_mate, x)
     piece(far_mate, x, False)
+    pass_diag(nz - 1)
     all_in(mate, 1 - x)
     piece(mate, 1 - x, False)
     piece(far, 1 - x, False)
@@ -1263,21 +1266,22 @@
         hid[xs * nz * cap : (xs + 1) * nz * cap] = (value / (1.0 + jnp.exp(-value)) * up[xs] * weight).astype(BF16)
     loads[2].wait()
 
-    def down(t):
+    def down(t, xs):
         at = pl.ds(pl.multiple_of(t * cols, 128), cols)
-        result = jnp.dot(hid[...], wd[:, at], preferred_element_type=F32)
-        return result.astype(BF16).reshape(nx, nz, cap, cols)
+        part = hid[pl.ds(pl.multiple_of(xs * (nz * cap), 16), nz * cap), :]
+        result = jnp.dot(part, wd[:, at], preferred_element_type=F32)
+        return result.astype(BF16).reshape(nz, cap, cols)
 
     def d_copy(k, xs):
         return remote(away.at[k, xs], arrived.at[k, xs], d_send.at[k, xs], d_recv.at[k, xs], to_mate)
 
-    away[1] = down(far_mate)
+    away[1, 1 - x] = down(far_mate, 1 - x)
     d_copy(1, 1 - x).start()
+    home[1, 1 - x] = down(far, 1 - x)
+    away[0, 1 - x] = down(mate, 1 - x)
+    d_copy(0, 1 - x).start()
+    away[1, x] = down(far_mate, x)
     d_copy(1, x).start()
-    away[0] = down(mate)
-    d_copy(0, 1 - x).start()
-    d_copy(0, x).start()
-    home[1] = down(far)
 
     def pair(k, xs, g):
         return home[k, xs, g].astype(F32) + arrived[k, xs, g].astype(F32)
@@ -1335,13 +1339,16 @@
     d_copy(1, 1 - x).wait_recv()
     for i in order:
         diagonal(i)
-    home[0] = down(tp)
+    home[0, 1 - x] = down(tp, 1 - x)
+    home[1, x] = down(far, x)
     d_copy(1, x).wait_recv()
     d_copy(0, 1 - x).wait_recv()
     for i in order[: nz // 2]:
         plain(i)
     for i in order[: nz // 2]:
         joined(i)
+    away[0, x] = down(mate, x)
+    d_copy(0, x).start()
     for i in late:
         plain(i)
     for i in late:
@@ -1351,6 +1358,7 @@
         g = near(i)
         return remote(outb.at[g], back.at[z], b_send.at[i], b_recv.at[z], {"sp": g * nx + x, "tp": tp})
 
+    home[0, x] = down(tp, x)
     d_copy(0, x).wait_recv()
     for i in order:
         g = near(i)

time: 79.1 us -> 76.8 us (0.971)
  Pallas kernels: 77.4 us -> 75.1 us
    pallas_call x1, Pallas kernels: 77.4 us -> 75.1 us  [body(): pl.pallas_call(kernel, out_shape=jax.ShapeDtypeStruct((rows, cols), BF16)...]
where the time goes in v5:
time: 76.8 us; the launch traced here: 76.6 us
  Pallas kernels  75.1 us (98%)
  local copies, waits for them, and re-layouts  1.57 us (2%)
    pallas_call x1, Pallas kernels, body(): pl.pallas_call(kernel, out_shape=jax.ShapeDtypeStruct((rows, cols), BF16)...  75.1 us
    unnamed x1, local copies, waits for them, and re-layouts  1.57 us

profile of v5, /device:TPU:0, one launch (start us, length us, event | category | flops | bytes accessed | tf_op | source)
XLA Modules:
  0.0 76.6 jit_solution(5062606821356536398)
XLA Ops:
  0.0 75.1 %shard_map.190 = bf16[128,512]{1,0:T(8,128)(2,1)} custom-call(bf16[128,512]{1,0:T(8,128)(2,1)} %refs_0_.1, bf16[128,512]{1,0:T(8,128)(2,1)} %refs_1_.1, bf16[512,128]{1,0:T(8,128)(2,1)} %bitcast.17, bf16[1024,128]{1,0:T(8,128)(2,1)} %bitcast.16, f32[8,128]{1,0:T(8,128)} %bitcast.18, f32[4,128]{1,0:T(4,128)} %bitcast.19, bf16[128,512]{1,0:T(8,128)(2,1)} %refs_6_.1, ...), custom_call_target="tpu_custom_call" | custom-call | tf_op jit(solution)/shard_map/pallas_call | solution.py:1654
  75.1 1.6 %copy.23 = bf16[128,512]{1,0:T(8,128)(2,1)} copy(bf16[128,512]{1,0:T(8,128)(2,1)} %shard_map.190) | data formatting | bytes 262144
